TPU v7x, 512 devices: a whole 4x4x16 slice. The times are simulated.
512 devices in a mesh: sp: 64 (over z, y), tp: 8 (over x, core).
Axes of the slice: x: 4, y: 4, z: 16, core: 2. Of those that a mesh axis runs over, the one named last changes fastest.
Arguments:
- queries: bfloat16 [8192, 1024], P('sp', 'tp'), may hold values from -5 to 5
- keys: bfloat16 [8192, 1024], P('sp', 'tp'), may hold values from -5 to 5
- values: bfloat16 [8192, 1024], P('sp', 'tp'), may hold values from -5 to 5
- in_gate: float32 [8, 8192], P('tp', 'sp'), may hold values from -7 to 213
- forget_gate: float32 [8, 8192], P('tp', 'sp'), may hold values from 0 to 17
- stream: bfloat16 [8192, 2048], P('sp', 'tp'), may hold values from -24 to 24
- head_gain: float32 [1024], replicated, may hold values from 0.1 to 1.9
- out_weight: bfloat16 [1024, 2048], P(None, 'tp'), may hold values from -0.1875 to 0.1875
- norm_gain: float32 [2048], replicated, may hold values from 0.1 to 1.9
- gate_weight: bfloat16 [2048, 5632], P('sp', 'tp'), may hold values from -0.125 to 0.125
- up_weight: bfloat16 [2048, 5632], P('sp', 'tp'), may hold values from -0.125 to 0.125
- down_weight: bfloat16 [2048, 5632], P('sp', 'tp'), may hold values from -0.15625 to 0.15625
Outputs:
- layer_out: float32 [8192, 2048], P('sp', 'tp')
All inputs are finite; a program needn't handle non-finite values.
Results may differ from a plain program's by a relative error of at most 0.004.
Values may be sent and summed in bfloat16 or wider, within the bound.
A program may use at most 64 MiB of HBM per device.

v0:
```python
import jax
import jax.numpy as jnp
from jax import lax
from jax.sharding import Mesh
from jax.sharding import PartitionSpec as P

HEAD_DIM = 128
BLOCK = 128
SP = ("sp_0", "sp_1")


norm_eps = 1e-06
far_below = -1e30


def filled_with(array, identity):
    return jax.tree.map(
        lambda part, zero: jnp.zeros_like(part) + jnp.asarray(zero, part.dtype), array, identity
    )


def collected_together(array, axis):
    leaves = jax.tree.leaves(array)
    order = sorted(range(len(leaves)), key=lambda k: -leaves[k].size)
    width = (1, *leaves[order[0]].shape)[-1]
    lines = [
        jnp.pad(leaves[k].reshape(-1), (0, -leaves[k].size % width)).reshape(-1, width)
        for k in order
    ]
    both, at, found = (lax.all_gather(jnp.concatenate(lines), axis), 0, {})
    for k, line in zip(order, lines):
        piece = both[:, at : at + len(line)].reshape(len(both), -1)
        found[k] = piece[:, : leaves[k].size].reshape(-1, *leaves[k].shape)
        at += len(line)
    numbers = iter(range(len(leaves)))
    return jax.tree.map(lambda _: found[next(numbers)], array)


def carried_in(array, axes, combine, identity):
    before = start = filled_with(array, identity)
    total = array
    for axis in reversed(axes):
        devices, here = (lax.axis_size(axis), lax.axis_index(axis))
        pieces = collected_together(total, axis)
        inside, total = (start, start)
        for k in range(devices):
            passed = k < here
            total = combine(total, jax.tree.map(lambda part: part[k], pieces))
            inside = jax.tree.map(lambda new, old: jnp.where(passed, new, old), total, inside)
        before = combine(inside, before)
    return before


def sent_together(arrays, axis, dim, along):
    widths = [a.shape[along] for a in arrays]
    both = jnp.concatenate(arrays, axis=along)
    filled = lax.all_gather(both, axis, axis=dim, tiled=True)
    return tuple(jnp.split(filled, [sum(widths[:k]) for k in range(1, len(widths))], axis=along))


def copy_for_each(array, axis):
    copies = jnp.broadcast_to(array, (lax.axis_size(axis), *array.shape))
    return lax.all_to_all(copies, axis, split_axis=0, concat_axis=0, tiled=True)


def joined_along(blocks, dim):
    shape = list(blocks.shape[1:])
    shape[dim] *= blocks.shape[0]
    return jnp.moveaxis(blocks, 0, dim).reshape(shape)


def collect(array, axis, dim):
    blocks = copy_for_each(array, axis)
    return joined_along(blocks, dim)


def in_blocks(array, dim, devices):
    shape = array.shape
    blocks = array.reshape(*shape[:dim], devices, shape[dim] // devices, *shape[dim + 1 :])
    return jnp.moveaxis(blocks, dim, 0)


def summed_on_arrival(array, axis, dim):
    devices = lax.axis_size(axis)
    blocks = lax.all_to_all(in_blocks(array, dim, devices), axis, 0, 0, tiled=True)
    return jnp.sum(blocks.astype(jnp.float32), axis=0)


def merge_states(earlier, later):
    memory_early, top_early, fall_early = earlier
    memory_late, top_late, fall_late = later
    new_top = jnp.maximum(fall_late + top_early, top_late)
    keep_early = jnp.exp(fall_late + top_early - new_top)
    keep_late = jnp.exp(top_late - new_top)
    memory = keep_early[..., None, None] * memory_early + keep_late[..., None, None] * memory_late
    return (memory, new_top, fall_early + fall_late)


def memory_cell(queries, keys, values, in_gate, forget_gate, own_gain):
    tokens = queries.shape[0]
    local_heads = in_gate.shape[0]
    blocks = tokens // BLOCK
    key_scale = HEAD_DIM ** (-0.5)
    query_blocks = queries.reshape(blocks, BLOCK, local_heads, HEAD_DIM)
    key_blocks = keys.reshape(blocks, BLOCK, local_heads, HEAD_DIM)
    value_blocks = values.reshape(blocks, BLOCK, local_heads, HEAD_DIM)
    gate_blocks = in_gate.reshape(local_heads, blocks, BLOCK)
    cumulative = jnp.cumsum(
        jax.nn.log_sigmoid(forget_gate).reshape(local_heads, blocks, BLOCK), axis=-1
    )
    block_fall = cumulative[..., -1]
    log_weight = block_fall[..., None] - cumulative + gate_blocks
    block_top = jnp.max(log_weight, axis=-1)
    key_weight = jnp.exp(log_weight - block_top[..., None]) * key_scale
    weighted = (jnp.transpose(key_weight, (1, 2, 0))[..., None] * key_blocks).astype(jnp.bfloat16)
    block_memory = jnp.einsum(
        "nshd,nshe->nhde", weighted, value_blocks, preferred_element_type=jnp.float32
    )
    neutral = (
        jnp.zeros((local_heads, HEAD_DIM, HEAD_DIM), jnp.float32),
        jnp.full((local_heads,), far_below, jnp.float32),
        jnp.zeros((local_heads,), jnp.float32),
    )

    def advance(running, summary):
        return (merge_states(running, summary), running)

    device_total, before_block = lax.scan(
        advance, neutral, (block_memory, block_top.T, block_fall.T)
    )
    incoming = carried_in(device_total, SP, merge_states, neutral)
    start_state = (
        jnp.zeros((local_heads, HEAD_DIM, HEAD_DIM), jnp.float32),
        jnp.zeros((local_heads,), jnp.float32),
        jnp.zeros((local_heads,), jnp.float32),
    )
    entering = merge_states(start_state, incoming)
    memory_in, top_in, fall_in = merge_states(
        jax.tree.map(lambda member: member[None], entering), before_block
    )
    causal = lax.broadcasted_iota(jnp.int32, (BLOCK, BLOCK), 0) >= lax.broadcasted_iota(
        jnp.int32, (BLOCK, BLOCK), 1
    )
    spread = cumulative[..., :, None] - cumulative[..., None, :] + gate_blocks[..., None, :]
    spread = jnp.where(causal, spread, -jnp.inf)
    carried = cumulative + top_in.T[..., None]
    row_top = jnp.maximum(carried, jnp.max(spread, axis=-1))
    decay_weight = jnp.exp(spread - row_top[..., None])
    scores = jnp.einsum(
        "nthd,nshd->hnts", query_blocks, key_blocks, preferred_element_type=jnp.float32
    )
    weights = (scores * key_scale * decay_weight).astype(jnp.bfloat16)
    inner_part = jnp.einsum(
        "hnts,nshe->nthe", weights, value_blocks, preferred_element_type=jnp.float32
    )
    outer_part = jnp.einsum(
        "nthd,nhde->nthe",
        query_blocks.astype(jnp.float32),
        memory_in,
        precision=lax.Precision.HIGHEST,
    )
    readout = (
        jnp.transpose(jnp.exp(carried - row_top), (1, 2, 0))[..., None] * outer_part + inner_part
    )
    row_scale = lax.rsqrt(jnp.mean(readout * readout, axis=-1, keepdims=True) + norm_eps)
    head_scale = own_gain.reshape(local_heads, HEAD_DIM)
    normed_heads = (readout * row_scale * head_scale).astype(jnp.bfloat16)
    return normed_heads.reshape(tokens, local_heads * HEAD_DIM)


def local(
    queries,
    keys,
    values,
    in_gate,
    forget_gate,
    stream,
    head_gain,
    out_weight,
    norm_gain,
    gate_weight,
    up_weight,
    down_weight,
):
    whole_gate, whole_up, whole_down = sent_together(
        (gate_weight, up_weight, down_weight), SP, 0, 1
    )
    column_index = lax.axis_index("tp")
    local_width = queries.shape[1]
    own_gain = lax.dynamic_slice_in_dim(head_gain, column_index * local_width, local_width)
    heads_out = memory_cell(queries, keys, values, in_gate, forget_gate, own_gain)
    projected = jnp.dot(collect(heads_out, "tp", 1), out_weight, preferred_element_type=jnp.float32)
    mixed_stream = stream.astype(jnp.float32) + projected
    whole_rows = collect(mixed_stream, "tp", 1)
    factor = lax.rsqrt(jnp.mean(whole_rows * whole_rows, axis=1, keepdims=True) + norm_eps)
    normed = (whole_rows * factor * norm_gain).astype(jnp.bfloat16)
    gate_acts = jnp.dot(normed, whole_gate, preferred_element_type=jnp.float32)
    up_acts = jnp.dot(normed, whole_up, preferred_element_type=jnp.float32)
    hidden = (jax.nn.silu(gate_acts) * up_acts).astype(jnp.bfloat16)
    channel = summed_on_arrival(
        jnp.einsum("df,tf->dt", whole_down, hidden, preferred_element_type=jnp.float32).astype(
            jnp.bfloat16
        ),
        "tp",
        0,
    )
    return mixed_stream + 0.5 * channel.T


def solution(mesh):
    finer = Mesh(mesh.devices.reshape(16, 4, mesh.shape["tp"]), ("sp_0", "sp_1", "tp"))
    in_specs = (
        P(SP, "tp"),
        P(SP, "tp"),
        P(SP, "tp"),
        P("tp", SP),
        P("tp", SP),
        P(SP, "tp"),
        P(),
        P(None, "tp"),
        P(),
        P(SP, "tp"),
        P(SP, "tp"),
        P(SP, "tp"),
    )
    out_specs = P(SP, "tp")
    return jax.shard_map(local, mesh=finer, in_specs=in_specs, out_specs=out_specs, check_vma=False)
```

profile of v0, /device:TPU:1, one launch (start us, length us, event | category | flops | bytes accessed | tf_op | source)
XLA Modules:
  0.0 305.6 jit_solution(16874232768643324905)
XLA Ops:
  6.5 0.0 copy-start
  6.5 0.0 copy-start.1
  6.5 0.0 all-gather.9.cloned.1.call-start
  6.5 0.7 fusion.193
  7.3 0.3 reduce_window_sum.13
  7.6 0.6 slice.281
  8.2 1.9 fusion.192
  11.8 1.9 exponential_multiply_fusion
  13.7 0.7 pad_bitcast_fusion.2
  14.5 1.0 fusion.18
  15.5 10.7 %all-gather.2 = f32[4,130,128]{2,1,0:T(8,128)S(1)} all-gather(f32[1,130,128]{2,1,0:T(8,128)S(1)} %maximum_bitcast_fusion), channel_id=2, replica_groups=mesh['sp_0'=16,'sp_1'=4,'tp'=8] {'sp_1'}, dimensions={0}, use_global_device_ids=true | all-gather | bytes 332800 | tf_op jit(solution)/shard_map/all_gather | solution.py:30
  26.3 0.6 fusion.203
  27.5 0.6 fusion.202
  37.7 0.6 maximum_bitcast_fusion.1
  38.3 0.0 all-gather.9.cloned.1.call-update
  38.4 0.0 all-gather.7.cloned.1.call-start
  38.4 1.6 concatenate.11
  40.0 0.0 all-gather.7.cloned.1.call-update
  40.8 0.8 dynamic_slice.11
  41.6 0.8 fusion.114
  42.4 63.3 %all-gather.9.cloned.1.call-done = f32[16,130,128]{2,1,0:T(8,128)} async-done(((f32[1,130,128]{2,1,0:T(8,128)}), f32[16,130,128]{2,1,0:T(8,128)}) %all-gather.9.cloned.1.call-update) | async-done | bytes 1064976 | tf_op jit(solution)/shard_map/all_gather | solution.py:30
  105.7 0.9 fusion.198
  106.6 0.7 fusion.201
  108.7 0.6 fusion.200
  149.9 1.1 convolution_bitcast_fusion
  151.0 1.8 multiply_reduce_fusion
  152.8 0.1 fusion.117
  152.9 0.0 copy-start.2
  153.0 21.5 %all_to_all.15 = bf16[8,128,128]{1,2,0:T(8,128)(2,1)S(1)} all-to-all(bf16[8,128,128]{1,2,0:T(8,128)(2,1)S(1)} %broadcast_in_dim.24), channel_id=1, replica_groups=mesh['sp_0'=16,'sp_1'=4,'tp'=8] {'tp'}, dimensions={0} | all-to-all | bytes 524288 | tf_op jit(solution)/shard_map/all_to_all | solution.py:63
  174.4 0.0 copy-done
  174.4 0.0 copy-done.1
  174.4 0.3 convolution_add_fusion
  174.7 0.1 copy.15
  174.8 0.1 broadcast_in_dim.25
  174.9 18.4 %all_to_all.16 = f32[8,128,256]{1,2,0:T(8,128)S(1)} all-to-all(f32[8,128,256]{1,2,0:T(8,128)S(1)} %broadcast_in_dim.25), channel_id=1, replica_groups=mesh['sp_0'=16,'sp_1'=4,'tp'=8] {'tp'}, dimensions={0} | all-to-all | bytes 2097152 | tf_op jit(solution)/shard_map/all_to_all | solution.py:63
  193.3 0.3 fusion.24
  193.6 0.0 copy-done.2
  193.6 0.3 fusion.23
  193.9 72.2 %all-gather.7.cloned.1.call-done = bf16[2048,2112]{1,0:T(8,128)(2,1)} async-done(((bf16[32,2112]{1,0:T(8,128)(2,1)}), bf16[2048,2112]{1,0:T(8,128)(2,1)}) %all-gather.7.cloned.1.call-update) | async-done | bytes 8650768 | tf_op jit(solution)/shard_map/all_gather | solution.py:57
  266.1 3.2 %fusion.2 = f32[128,704]{0,1:T(8,128)S(1)} fusion(bf16[128,2048]{0,1:T(8,128)(2,1)S(1)} %fusion.23, bf16[2048,2112]{1,0:T(8,128)(2,1)} %all-gather.7.cloned.1.call-done), kind=kOutput, calls=%fused_computation.2 | convolution fusion | flops 369098752 | bytes 4030464 | tf_op jit(solution)/shard_map/dot_general | solution.py:197
  269.3 7.0 %fusion.6 = bf16[2048,128]{1,0:T(8,128)(2,1)S(1)} fusion(bf16[2048,2112]{1,0:T(8,128)(2,1)} %all-gather.7.cloned.1.call-done, bf16[128,2048]{0,1:T(8,128)(2,1)S(1)} %fusion.23, f32[128,704]{0,1:T(8,128)S(1)} %fusion.2), kind=kOutput, calls=%fused_computation.6 | convolution fusion | flops 739000320 | bytes 7700480 | tf_op jit(solution)/shard_map/df,tf->dt/dot_general | solution.py:201
  276.3 21.6 %all_to_all.17 = bf16[8,256,128]{2,1,0:T(8,128)(2,1)S(1)} all-to-all(bf16[8,256,128]{2,1,0:T(8,128)(2,1)S(1)} %bitcast.193), channel_id=1, replica_groups=mesh['sp_0'=16,'sp_1'=4,'tp'=8] {'tp'}, dimensions={0} | all-to-all | bytes 1048576 | tf_op jit(solution)/shard_map/all_to_all | solution.py:85
  298.0 0.1 convert_reduce_fusion
  298.0 0.1 copy.16
  298.1 0.7 bitcast_add_fusion
  (9 shorter events, 0.1 us)
Async XLA Ops:
  6.5 167.9 %copy-start = (bf16[1024,256]{1,0:T(8,128)(2,1)S(1)}, bf16[1024,256]{1,0:T(8,128)(2,1)}, u32[]{:S(2)}) copy-start(bf16[1024,256]{1,0:T(8,128)(2,1)} %param.19) | copy-start | bytes 1572868
  6.5 167.9 %copy-start.1 = (bf16[128,256]{1,0:T(8,128)(2,1)S(1)}, bf16[128,256]{1,0:T(8,128)(2,1)}, u32[]{:S(2)}) copy-start(bf16[128,256]{1,0:T(8,128)(2,1)} %param.17) | copy-start | bytes 196612
  6.5 99.1 %all-gather.9.cloned.1.call-start = ((), (), s32[]{:S(2)}) async-start(), calls=%async_computation.4 | async-start | bytes 1183744 | tf_op jit(solution)/shard_map/all_gather | solution.py:30
  38.4 227.7 %all-gather.7.cloned.1.call-start = ((), (), s32[]{:S(2)}) async-start(), calls=%async_computation.3 | async-start | bytes 9052160 | tf_op jit(solution)/shard_map/all_gather | solution.py:57
  152.9 40.7 %copy-start.2 = (f32[2048]{0:T(1024)S(1)}, f32[2048]{0:T(1024)}, u32[]{:S(2)}) copy-start(f32[2048]{0:T(1024)} %param.20) | copy-start | bytes 24580
Sparse Core Ops, SparseCore 0:
  38.5 67.1 all-gather.8
  108.6 157.4 all-gather.6
where the time goes:
time: 307 us; the launch traced here: 306 us
  waiting for transfers between devices  136 us (44%)
  blocking collectives  72.3 us (24%)
  between operations  68.3 us (22%)
  matrix products  14.4 us (5%)
  other arithmetic  7.8 us (3%)
  local copies, waits for them, and re-layouts  7.33 us (2%)
    all_gather x1, waiting for transfers between devices, sent_together(): filled = lax.all_gather(both, axis, axis=dim, tiled=True)  72.2 us
    all_gather x1, waiting for transfers between devices, collected_together(): both, at, found = (lax.all_gather(jnp.concatenate(lines), axis), 0, {})  63.3 us
    all_to_all x2, blocking collectives, copy_for_each(): return lax.all_to_all(copies, axis, split_axis=0, concat_axis=0, tiled=True)  39.9 us
    all_to_all x1, blocking collectives, summed_on_arrival(): lax.all_to_all(in_blocks(array, dim, devices), axis, 0, 0, tiled=True)  21.6 us
    all_gather x1, blocking collectives, collected_together(): both, at, found = (lax.all_gather(jnp.concatenate(lines), axis), 0, {})  10.7 us
    dot_general x1, matrix products, local(): jnp.einsum('df,tf->dt', whole_down, hidden, preferred_element_type=jnp.fl...  7.01 us
  transfers between devices with their start and end apart: 2, of which 2 were waited for; matrix products, arithmetic and copies ran while one was open for 3% of the time, Pallas kernels for 0%

commit v1 on v0

v1 whole, which is shorter than its diff:
```python
import functools

import jax
import jax.numpy as jnp
from jax import lax
from jax.experimental import pallas as pl
from jax.experimental.pallas import tpu as pltpu
from jax.sharding import Mesh
from jax.sharding import PartitionSpec as P

MESH = pl.DeviceIdType.MESH
F32 = jnp.float32
BF16 = jnp.bfloat16

T = 128
WIDE = 256
UNITS = 176
EPS = 1e-6
FAR = -1e30


def dot(a, b):
    return jnp.dot(a, b, preferred_element_type=F32)


def merge(early, late):
    memory_e, top_e, fall_e = early
    memory_l, top_l, fall_l = late
    top = jnp.maximum(fall_l + top_e, top_l)
    memory = jnp.exp(fall_l + top_e - top) * memory_e + jnp.exp(top_l - top) * memory_l
    return memory, top, fall_e + fall_l


def three_pieces(a):
    high = a.astype(BF16).astype(F32)
    rest = a - high
    middle = rest.astype(BF16).astype(F32)
    return high, middle, rest - middle


def kernel(
    nz,
    ny,
    nx,
    q_ref,
    k_ref,
    v_ref,
    in_ref,
    forget_ref,
    stream_ref,
    head_gain_ref,
    out_w_ref,
    norm_gain_ref,
    gate_w_ref,
    up_w_ref,
    down_w_ref,
    out_ref,
    tail,
    gu_pack,
    d_pack,
    d_block,
    w_gu,
    w_d,
    w_d2,
    m_send,
    m_got,
    z_send,
    z_got,
    e_send,
    e_got,
    heads,
    mixed_ref,
    acts,
    squares,
    hidden,
    r_send,
    r_got,
    ya_s,
    ya_r,
    z_s,
    z_r,
    e_s,
    e_r,
    ring_s,
    ring_r,
    h_s,
    h_r,
    a_s,
    a_r,
    p_s,
    p_r,
    d2_s,
    d2_r,
    x_s,
    x_r,
    r_s,
    r_r,
):
    z, y, x, c = (lax.axis_index(a) for a in ("z", "y", "x", "c"))
    tp = x * 2 + c
    n_tp = 2 * nx
    other = 1 - c

    def remote(src, dst, send, recv, **where):
        return pltpu.make_async_remote_copy(
            src_ref=src,
            dst_ref=dst,
            send_sem=send,
            recv_sem=recv,
            device_id=where,
            device_id_type=MESH,
        )

    def arrived(dst, send, recv):
        remote(dst, dst, send, recv, c=other).wait_recv()

    barrier = pltpu.get_barrier_semaphore()

    def greet(**where):
        pl.semaphore_signal(barrier, inc=1, device_id=where, device_id_type=MESH)

    for dz in range(1, nz):
        greet(z=lax.rem(z + dz, nz))
    plane = [(dx, dy) for dx in range(nx) for dy in range(ny)]
    for dx, dy in plane:
        for dc in range(2):
            if dx or dy or dc:
                greet(x=lax.rem(x + dx, nx), y=lax.rem(y + dy, ny), c=lax.rem(c + dc, 2))

    rows = lax.broadcasted_iota(jnp.int32, (T, T), 0)
    lanes = lax.broadcasted_iota(jnp.int32, (T, T), 1)
    causal = rows >= lanes
    same = rows == lanes
    forget = forget_ref[...]
    fall_each = jnp.minimum(forget, 0.0) - jnp.log1p(jnp.exp(-jnp.abs(forget)))
    in_row = in_ref[...]

    def column(row):
        return jnp.sum(jnp.where(same, jnp.broadcast_to(row, (T, T)), 0.0), axis=1, keepdims=True)

    fall_column = column(fall_each)
    in_column = column(in_row)
    cum_column = jnp.sum(
        jnp.where(causal, jnp.broadcast_to(fall_each, (T, T)), 0.0), axis=1, keepdims=True
    )
    cum_row = jnp.sum(
        jnp.where(rows <= lanes, jnp.broadcast_to(fall_column, (T, T)), 0.0), axis=0, keepdims=True
    )
    fall = jnp.broadcast_to(jnp.sum(fall_each, axis=1, keepdims=True), (1, T))
    log_weight = jnp.broadcast_to(fall - cum_column + in_column, (T, T))
    top = jnp.max(log_weight, axis=0, keepdims=True)
    weighted = jnp.exp(log_weight - top) * (T**-0.5) * k_ref[...].astype(F32)
    memory = lax.dot_general(
        weighted.astype(BF16), v_ref[...], (((0,), (0,)), ((), ())), preferred_element_type=F32
    )
    slice_rows = T // ny
    sub8 = lax.broadcasted_iota(jnp.int32, (8, T), 0)
    for j in range(ny):
        m_send[j, 0:slice_rows] = memory[j * slice_rows : (j + 1) * slice_rows]
        m_send[j, slice_rows : slice_rows + 8] = jnp.where(
            sub8 == 0, top, jnp.where(sub8 == 1, fall, 0.0)
        )
    m_got[y] = m_send[y]

    shard = gate_w_ref.shape[0]
    lane = lax.broadcasted_iota(jnp.int32, (shard, T), 1)
    ends = []
    for n, ref in enumerate((gate_w_ref, up_w_ref, down_w_ref)):
        tail[n] = jnp.zeros((shard, T), F32)
        tail[n, :, 0:64] = ref[:, 640:704].astype(F32)
        ends.append((ref[:, 512:640].astype(F32), tail[n]))

    def rest_of(n, j, at):
        wide, narrow = ends[n]
        wide = pltpu.roll(wide, (at - 32 * j) % T, 1)
        narrow = pltpu.roll(narrow, (at + 32 - 16 * j) % T, 1)
        here = (lane >= at) & (lane < at + 48)
        return jnp.where(here, jnp.where(lane < at + 32, wide, narrow), 0.0)

    for j in range(ny):
        gu_pack[j, :, 0:128] = gate_w_ref[:, j * T : (j + 1) * T]
        gu_pack[j, :, 128:256] = up_w_ref[:, j * T : (j + 1) * T]
        gu_pack[j, :, 256:384] = (rest_of(0, j, 0) + rest_of(1, j, 64)).astype(BF16)
        d_pack[j, :, 0:128] = down_w_ref[:, j * T : (j + 1) * T]
        d_pack[j, :, 128:256] = rest_of(2, j, 0).astype(BF16)

    def gu_rows(slot, begin, count):
        return w_gu.at[slot // 2, pl.ds(pl.multiple_of((slot % 2) * T + begin, 32), count), :]

    own_rows = pl.ds(pl.multiple_of((z % 2) * T + y * shard, 32), shard)
    w_gu[z // 2, own_rows, :] = gu_pack[y]
    d_block[pl.ds(pl.multiple_of(y * shard, 32), shard), :] = d_pack[y]
    for s in range(nz):
        w_d[s, UNITS:256] = jnp.zeros((256 - UNITS, T), BF16)
    for s in range(nz // 2):
        w_d2[s, UNITS:256] = jnp.zeros((256 - UNITS, T), BF16)

    pl.semaphore_wait(barrier, nz - 1 + 2 * nx * ny - 1)

    sent = []

    def send(*args, **where):
        copy = remote(*args, **where)
        copy.start()
        sent.append(copy)

    for dy in range(1, ny):
        to = lax.rem(y + dy, ny)
        send(m_send.at[to], m_got.at[y], ya_s.at[0, dy], ya_r.at[0, dy], y=to)
    for dy in range(1, ny):
        to = lax.rem(y + dy, ny)
        send(gu_pack.at[to], gu_rows(z, y * shard, shard), ya_s.at[1, dy], ya_r.at[1, dy], y=to)
        d_rows = pl.ds(pl.multiple_of(y * shard, 32), shard)
        send(d_pack.at[to], d_block.at[d_rows], ya_s.at[2, dy], ya_r.at[2, dy], y=to)

    scores = lax.dot_general(
        q_ref[...], k_ref[...], (((1,), (1,)), ((), ())), preferred_element_type=F32
    ) * (T**-0.5)

    for dy in range(1, ny):
        arrived(m_got.at[lax.rem(y + ny - dy, ny)], ya_s.at[0, dy], ya_r.at[0, dy])
    state = (jnp.zeros((slice_rows, T), F32), jnp.full((1, T), FAR, F32), jnp.zeros((1, T), F32))
    before = []
    for j in range(ny):
        before.append(state)
        got = m_got[j]
        late = (
            got[0:slice_rows],
            got[slice_rows : slice_rows + 1],
            got[slice_rows + 1 : slice_rows + 2],
        )
        state = merge(state, late)
    plane_memory, plane_top, plane_fall = state
    sub16 = lax.broadcasted_iota(jnp.int32, (16, T), 0)
    numbers = jnp.zeros((16, T), F32)
    for n, piece in enumerate((*three_pieces(plane_top), *three_pieces(plane_fall))):
        numbers = jnp.where(sub16 == n, piece, numbers)
    z_send[0:slice_rows] = plane_memory.astype(BF16)
    z_send[slice_rows : slice_rows + 16] = numbers.astype(BF16)
    for dz in range(nz - 1, 0, -1):

        @pl.when(z + dz < nz)
        def _():
            remote(z_send, z_got.at[dz], z_s.at[dz], z_r.at[dz], z=z + dz).start()

    up_z, down_z = lax.rem(z + 1, nz), lax.rem(z + nz - 1, nz)
    rounds = nz // 2

    def ring_parts(n, slot, r, **where):
        return (
            remote(
                gu_rows(slot, 0, T),
                gu_rows(slot, 0, T),
                ring_s.at[n, 0, r],
                ring_r.at[n, 0, r],
                **where,
            ),
            remote(
                w_d.at[slot, pl.ds(0, UNITS)],
                w_d.at[slot, pl.ds(0, UNITS)],
                ring_s.at[n, 1, r],
                ring_r.at[n, 1, r],
                **where,
            ),
        )

    def ring_start(r):
        for copy in ring_parts(0, lax.rem(z + nz - r + 1, nz), r, z=up_z):
            copy.start()
            sent.append(copy)
        if r < rounds:
            for copy in ring_parts(1, lax.rem(z + r - 1, nz), r, z=down_z):
                copy.start()
                sent.append(copy)

    def ring_wait(r):
        for copy in ring_parts(0, lax.rem(z + nz - r, nz), r, z=up_z):
            copy.wait_recv()
        if r < rounds:
            for copy in ring_parts(1, lax.rem(z + r, nz), r, z=down_z):
                copy.wait_recv()

    def ring_turn(r):
        ring_wait(r)
        if r < rounds:
            ring_start(r + 1)

    for dy in range(1, ny):
        by = lax.rem(y + ny - dy, ny)
        arrived(gu_rows(z, by * shard, shard), ya_s.at[1, dy], ya_r.at[1, dy])
        d_rows = pl.ds(pl.multiple_of(by * shard, 32), shard)
        arrived(d_block.at[d_rows], ya_s.at[2, dy], ya_r.at[2, dy])
    turned = jnp.transpose(d_block[...].astype(F32))
    w_d[z, 0:UNITS] = turned[0:UNITS].astype(BF16)
    ring_start(1)

    def pass_plane(dz, carry):
        total, highest, fallen = carry
        arrived(z_got.at[dz], z_s.at[dz], z_r.at[dz])
        got = z_got[dz].astype(F32)
        found = got[slice_rows : slice_rows + 16]
        top_there = found[0:1] + found[1:2] + found[2:3]
        fall_there = found[3:4] + found[4:5] + found[5:6]
        level = top_there + fallen
        new = jnp.maximum(highest, level)
        total = total * jnp.exp(highest - new) + jnp.exp(level - new) * got[0:slice_rows]
        return total, new, fallen + fall_there

    total, highest, fallen = lax.fori_loop(
        1,
        z + 1,
        pass_plane,
        (jnp.zeros((slice_rows, T), F32), jnp.full((1, T), FAR, F32), jnp.zeros((1, T), F32)),
    )
    top_in = jnp.maximum(fallen, highest)
    plane_in = (total * jnp.exp(highest - top_in), top_in, jnp.zeros((1, T), F32))
    for j in range(ny):
        memory_j, top_j, _ = merge(plane_in, before[j])
        e_send[j, 0:slice_rows] = memory_j
        e_send[j, slice_rows : slice_rows + 8] = jnp.broadcast_to(top_j, (8, T))
    e_got[y] = e_send[y]
    for dy in range(1, ny):
        to = lax.rem(y + dy, ny)
        send(e_send.at[to], e_got.at[y], e_s.at[dy], e_r.at[dy], y=to)

    ring_turn(1)

    for dy in range(1, ny):
        arrived(e_got.at[lax.rem(y + ny - dy, ny)], e_s.at[dy], e_r.at[dy])

    memory_in = jnp.concatenate([e_got[j, 0:slice_rows] for j in range(ny)], axis=0)
    top_here = e_got[0, slice_rows : slice_rows + 1]
    cum_wide = jnp.broadcast_to(cum_column, (T, T))
    carried = cum_wide + top_here
    spread = jnp.where(causal, cum_wide - cum_row + in_row, -jnp.inf)
    row_top = jnp.maximum(carried, jnp.max(spread, axis=1, keepdims=True))
    block_weights = (scores * jnp.exp(spread - row_top)).astype(BF16)
    inner = dot(block_weights, v_ref[...])
    outer = sum(dot(q_ref[...], piece.astype(BF16)) for piece in three_pieces(memory_in))
    readout = jnp.exp(carried - row_top) * outer + inner
    scale = lax.rsqrt(jnp.mean(readout * readout, axis=1, keepdims=True) + EPS)
    normed_heads = (readout * scale * head_gain_ref[pl.ds(tp, 1), :]).astype(BF16)
    heads[tp] = normed_heads
    for d in range(1, n_tp):
        to = lax.rem(tp + d, n_tp)
        send(heads.at[tp], heads.at[tp], h_s.at[d], h_r.at[d], x=to // 2, c=to % 2)

    ring_turn(2)

    for d in range(1, n_tp):
        by = lax.rem(tp + n_tp - d, n_tp)
        arrived(heads.at[by], h_s.at[d], h_r.at[d])
    mixed = stream_ref[...].astype(F32)
    for n in range(nx):
        pair = jnp.concatenate([heads[2 * n], heads[2 * n + 1]], axis=1)
        mixed = mixed + dot(pair, out_w_ref[n * WIDE : (n + 1) * WIDE, :])
    mixed_ref[...] = mixed
    own_tokens = pl.ds(pl.multiple_of(y * T, T), T)
    for half in range(2):
        gain = norm_gain_ref[pl.ds(2 * tp + half, 1), :]
        part = mixed[:, half * T : (half + 1) * T]
        acts[tp, own_tokens, half * T : (half + 1) * T] = (part * gain).astype(BF16)
    square_column = jnp.sum(mixed * mixed, axis=1, keepdims=True)
    square_row = jnp.sum(
        jnp.where(same, jnp.broadcast_to(square_column, (T, T)), 0.0), axis=0, keepdims=True
    )
    squares[tp, y] = jnp.broadcast_to(square_row, (8, T))

    def piece_of(tp_there, y_there):
        tokens = pl.ds(pl.multiple_of(y_there * T, T), T)
        return acts.at[tp_there, tokens, :], squares.at[tp_there, y_there]

    def pass_on(n):
        dx, dy = plane[n]
        tp_there = lax.rem(x + nx - dx, nx) * 2 + c
        for m, ref in enumerate(piece_of(tp_there, lax.rem(y + ny - dy, ny))):
            send(ref, ref, p_s.at[m, n], p_r.at[m, n], c=other)

    order = sorted(
        range(1, len(plane)), key=lambda n: sum(min(d, 4 - d) for d in plane[n])
    )
    for n in reversed(order):
        dx, dy = plane[n]
        for m, ref in enumerate(piece_of(tp, y)):
            send(
                ref,
                ref,
                a_s.at[m, n],
                a_r.at[m, n],
                x=lax.rem(x + dx, nx),
                y=lax.rem(y + dy, ny),
            )
    pass_on(0)
    for r in range(3, rounds + 1):
        ring_turn(r)

    for b in range(nx):
        for half in range(2):
            send(
                w_d.at[4 * b + 2 * other + half, pl.ds(0, UNITS)],
                w_d2.at[2 * b + half, pl.ds(0, UNITS)],
                d2_s.at[2 * b + half],
                d2_r.at[2 * b + half],
                c=other,
            )

    for n in order:
        dx, dy = plane[n]
        tp_there = lax.rem(x + nx - dx, nx) * 2 + c
        for m, ref in enumerate(piece_of(tp_there, lax.rem(y + ny - dy, ny))):
            arrived(ref, a_s.at[m, n], a_r.at[m, n])
        pass_on(n)
    for n in range(len(plane)):
        dx, dy = plane[n]
        tp_there = lax.rem(x + nx - dx, nx) * 2 + other
        for m, ref in enumerate(piece_of(tp_there, lax.rem(y + ny - dy, ny))):
            arrived(ref, p_s.at[m, n], p_r.at[m, n])

    lane_wide = lax.broadcasted_iota(jnp.int32, (T, T), 1)
    for j in range(ny):
        both = jnp.zeros((T, 3 * T), F32)
        total_square = jnp.zeros((1, T), F32)
        for b in range(n_tp):
            both = both + dot(acts[b, j * T : (j + 1) * T, :], w_gu[b])
            total_square = total_square + squares[b, j][0:1]
        factor = lax.rsqrt(column(total_square) * (1.0 / (n_tp * WIDE)) + EPS)
        both = both * factor
        gate, up, rest = both[:, 0:T], both[:, T : 2 * T], both[:, 2 * T : 3 * T]
        hidden[c, j * T : (j + 1) * T, 0:T] = (gate / (1.0 + jnp.exp(-gate)) * up).astype(BF16)
        small = rest / (1.0 + jnp.exp(-rest)) * pltpu.roll(rest, 64, 1)
        hidden[c, j * T : (j + 1) * T, T : 2 * T] = jnp.where(lane_wide < 48, small, 0.0).astype(
            BF16
        )
    send(hidden.at[c], hidden.at[c], x_s, x_r, c=other)

    for n in range(2 * nx):
        arrived(w_d2.at[n, pl.ds(0, UNITS)], d2_s.at[n], d2_r.at[n])
    arrived(hidden.at[other], x_s, x_r)

    for dx in (2, 1, 3, 0):
        b = lax.rem(x + dx, nx)
        own = jnp.concatenate([w_d[4 * b + 2 * c], w_d[4 * b + 2 * c + 1]], axis=1)
        theirs = jnp.concatenate([w_d2[2 * b], w_d2[2 * b + 1]], axis=1)
        r_send[dx] = (dot(hidden[c], own) + dot(hidden[other], theirs)).astype(BF16)
        for dy in (2, 1, 3, 0):
            if dx or dy:
                to = lax.rem(y + dy, ny)
                send(
                    r_send.at[dx, pl.ds(pl.multiple_of(to * T, T), T), :],
                    r_got.at[dx * ny + dy],
                    r_s.at[dx * ny + dy],
                    r_r.at[dx * ny + dy],
                    x=b,
                    y=to,
                )
    channel = r_send[0, own_tokens, :].astype(F32)
    for n in order:
        arrived(r_got.at[n], r_s.at[n], r_r.at[n])
        channel = channel + r_got[n].astype(F32)
    out_ref[...] = mixed_ref[...] + 0.5 * channel

    for dz in range(1, nz):

        @pl.when(z + dz < nz)
        def _():
            remote(z_send, z_got.at[dz], z_s.at[dz], z_r.at[dz], z=z + dz).wait_send()

    for copy in sent:
        copy.wait_send()


def local(nz, ny, nx, *args):
    queries, keys, values, in_gate, forget_gate, stream = args[:6]
    head_gain, out_weight, norm_gain, gate_weight, up_weight, down_weight = args[6:]
    n_tp = 2 * nx
    dma = pltpu.SemaphoreType.DMA
    vmem = pltpu.VMEM
    slice_rows = T // ny
    shard = gate_weight.shape[0]
    scratch = [
        vmem((3, shard, T), F32),
        vmem((ny, shard, 3 * T), BF16),
        vmem((ny, shard, 2 * T), BF16),
        vmem((T, 2 * T), BF16),
        vmem((nz // 2, 2 * T, 3 * T), BF16),
        vmem((nz, 256, T), BF16),
        vmem((nz // 2, 256, T), BF16),
        vmem((ny, slice_rows + 8, T), F32),
        vmem((ny, slice_rows + 8, T), F32),
        vmem((slice_rows + 16, T), BF16),
        vmem((nz, slice_rows + 16, T), BF16),
        vmem((ny, slice_rows + 8, T), F32),
        vmem((ny, slice_rows + 8, T), F32),
        vmem((n_tp, T, T), BF16),
        vmem((T, WIDE), F32),
        vmem((n_tp, ny * T, WIDE), BF16),
        vmem((n_tp, ny, 8, T), F32),
        vmem((2, ny * T, 2 * T), BF16),
        vmem((nx, ny * T, WIDE), BF16),
        vmem((nx * ny, T, WIDE), BF16),
    ]
    for shape in (
        (3, ny),
        (nz,),
        (ny,),
        (2, 2, nz // 2 + 1),
        (n_tp,),
        (2, nx * ny),
        (2, nx * ny),
        (2 * nx,),
        None,
        (nx * ny,),
    ):
        scratch += [dma if shape is None else dma(shape)] * 2
    return pl.pallas_call(
        functools.partial(kernel, nz, ny, nx),
        out_shape=jax.ShapeDtypeStruct((T, WIDE), F32),
        in_specs=[pl.BlockSpec(memory_space=vmem)] * 12,
        out_specs=pl.BlockSpec(memory_space=vmem),
        scratch_shapes=scratch,
        compiler_params=pltpu.CompilerParams(collective_id=0, has_side_effects=True),
        name="layer",
    )(
        queries,
        keys,
        values,
        in_gate,
        forget_gate,
        stream,
        head_gain.reshape(n_tp, T),
        out_weight,
        norm_gain.reshape(2 * n_tp, T),
        gate_weight,
        up_weight,
        down_weight,
    )


def solution(mesh):
    nz, ny, nx = 16, 4, mesh.shape["tp"] // 2
    finer = Mesh(mesh.devices.reshape(nz, ny, nx, 2), ("z", "y", "x", "c"))
    rows, columns = ("z", "y"), ("x", "c")
    in_specs = (
        P(rows, columns),
        P(rows, columns),
        P(rows, columns),
        P(columns, rows),
        P(columns, rows),
        P(rows, columns),
        P(),
        P(None, columns),
        P(),
        P(rows, columns),
        P(rows, columns),
        P(rows, columns),
    )
    return jax.shard_map(
        functools.partial(local, nz, ny, nx),
        mesh=finer,
        in_specs=in_specs,
        out_specs=P(rows, columns),
        check_vma=False,
    )
```

time: 307 us -> 97.5 us (0.32)
  waiting for transfers between devices: 136 us -> 0 us
  Pallas kernels: 0 us -> 95.8 us
  blocking collectives: 72.3 us -> 0 us
  between operations: 68.3 us -> 0.01 us
  matrix products: 14.4 us -> 0 us
  other arithmetic: 7.8 us -> 0 us
  local copies, waits for them, and re-layouts: 7.33 us -> 1.57 us
    all_gather x2 -> x0, waiting for transfers between devices: 135 us -> none  [the longest x1 72.2 us: sent_together(): filled = lax.all_gather(both, axis, axis=dim, tiled=True)]
    pallas_call x0 -> x1, Pallas kernels: none -> 95.8 us  [local(): pl.pallas_call(functools.partial(kernel, nz, ny, nx), out_shape=jax.Shape...]
    all_to_all x3 -> x0, blocking collectives: 61.5 us -> none  [the longest x2 39.9 us: copy_for_each(): return lax.all_to_all(copies, axis, split_axis=0, concat_axis=0, tiled=True)]
    dot_general x6 -> x0, matrix products: 14.4 us -> none  [the longest x1 7.01 us: local(): jnp.einsum('df,tf->dt', whole_down, hidden, preferred_element_type=jnp.fl...]
    all_gather x1 -> x0, blocking collectives: 10.7 us -> none  [collected_together(): both, at, found = (lax.all_gather(jnp.concatenate(lines), axis), 0, {})]
    slice x7 -> x0, local copies, waits for them, and re-layouts: 4 us -> none  [the longest x4 2.48 us: carried_in(): total = combine(total, jax.tree.map(lambda part: part[k], pieces))]
  transfers between devices with their start and end apart: 2 -> 0, of which waited for: 2 -> 0; matrix products, arithmetic and copies ran while one was open for 3% -> 0% of each run, Pallas kernels for 0% -> 0%
where the time goes in v1:
time: 97.5 us; the launch traced here: 97.4 us
  Pallas kernels  95.8 us (98%)
  local copies, waits for them, and re-layouts  1.57 us (2%)
    pallas_call x1, Pallas kernels, local(): pl.pallas_call(functools.partial(kernel, nz, ny, nx), out_shape=jax.Shape...  95.8 us

profile of v1, /device:TPU:1, one launch (start us, length us, event | category | flops | bytes accessed | tf_op | source)
XLA Modules:
  0.0 97.4 jit_solution(7048969644725778330)
XLA Ops:
  0.0 95.8 %layer.1 = f32[128,256]{1,0:T(8,128)} custom-call(bf16[128,128]{1,0:T(8,128)(2,1)} %q_ref.1, bf16[128,128]{1,0:T(8,128)(2,1)} %k_ref.1, bf16[128,128]{1,0:T(8,128)(2,1)} %v_ref.1, f32[1,128]{1,0:T(1,128)} %in_ref.1, f32[1,128]{1,0:T(1,128)} %forget_ref.1, bf16[128,256]{1,0:T(8,128)(2,1)} %stream_ref.1, f32[8,128]{1,0:T(8,128)} %bitcast.3, ...), custom_call_target="tpu_custom_call" | custom-call | tf_op jit(solution)/shard_map/layer/pallas_call | solution.py:515
  95.8 1.6 %copy.14 = f32[128,256]{1,0:T(8,128)} copy(f32[128,256]{1,0:T(8,128)} %layer.1) | data formatting | bytes 262144

commit v2 on v1

v2 whole, which is shorter than its diff:
```python
import functools

import jax
import jax.numpy as jnp
from jax import lax
from jax.experimental import pallas as pl
from jax.experimental.pallas import tpu as pltpu
from jax.sharding import Mesh
from jax.sharding import PartitionSpec as P

MESH = pl.DeviceIdType.MESH
F32 = jnp.float32
BF16 = jnp.bfloat16

T = 128
WIDE = 256
UNITS = 176
EPS = 1e-6
FAR = -1e30
SECTION = 4
TURNS = ((1, 1), (6, 6), (3, 3), (3, 3))
GROUPS = (2, 1, 3, 0)
RING_ROUNDS = (8, 7)


def dot(a, b):
    return jnp.dot(a, b, preferred_element_type=F32)


def merge(early, late):
    memory_e, top_e, fall_e = early
    memory_l, top_l, fall_l = late
    top = jnp.maximum(fall_l + top_e, top_l)
    memory = jnp.exp(fall_l + top_e - top) * memory_e + jnp.exp(top_l - top) * memory_l
    return memory, top, fall_e + fall_l


def three_pieces(a):
    high = a.astype(BF16).astype(F32)
    rest = a - high
    middle = rest.astype(BF16).astype(F32)
    return high, middle, rest - middle


def kernel(
    nz,
    ny,
    nx,
    q_ref,
    k_ref,
    v_ref,
    in_ref,
    forget_ref,
    stream_ref,
    head_gain_ref,
    out_w_ref,
    norm_gain_ref,
    gate_w_ref,
    up_w_ref,
    down_w_ref,
    out_ref,
    tail,
    gu_pack,
    d_pack,
    d_block,
    w_gu,
    w_d,
    w_d2,
    m_send,
    m_got,
    z_send,
    z_got,
    s_send,
    s_got,
    e_send,
    e_got,
    heads,
    mixed_ref,
    acts,
    squares,
    hidden,
    r_send,
    r_got,
    ya_s,
    ya_r,
    z_s,
    z_r,
    s_s,
    s_r,
    e_s,
    e_r,
    ring_s,
    ring_r,
    h_s,
    h_r,
    a_s,
    a_r,
    p_s,
    p_r,
    d2_s,
    d2_r,
    x_s,
    x_r,
    r_s,
    r_r,
):
    z, y, x, c = (lax.axis_index(a) for a in ("z", "y", "x", "c"))
    tp = x * 2 + c
    n_tp = 2 * nx
    other = 1 - c

    def remote(src, dst, send, recv, **where):
        return pltpu.make_async_remote_copy(
            src_ref=src,
            dst_ref=dst,
            send_sem=send,
            recv_sem=recv,
            device_id=where,
            device_id_type=MESH,
        )

    def arrived(dst, send, recv):
        remote(dst, dst, send, recv, c=other).wait_recv()

    barrier = pltpu.get_barrier_semaphore()

    def greet(**where):
        pl.semaphore_signal(barrier, inc=1, device_id=where, device_id_type=MESH)

    for dz in range(1, nz):
        greet(z=lax.rem(z + dz, nz))
    plane = [(dx, dy) for dx in range(nx) for dy in range(ny)]
    for dx, dy in plane:
        for dc in range(2):
            if dx or dy or dc:
                greet(x=lax.rem(x + dx, nx), y=lax.rem(y + dy, ny), c=lax.rem(c + dc, 2))

    rows = lax.broadcasted_iota(jnp.int32, (T, T), 0)
    lanes = lax.broadcasted_iota(jnp.int32, (T, T), 1)
    causal = rows >= lanes
    same = rows == lanes
    forget = forget_ref[...]
    fall_each = jnp.minimum(forget, 0.0) - jnp.log1p(jnp.exp(-jnp.abs(forget)))
    in_row = in_ref[...]

    def column(row):
        return jnp.sum(jnp.where(same, jnp.broadcast_to(row, (T, T)), 0.0), axis=1, keepdims=True)

    fall_column = column(fall_each)
    in_column = column(in_row)
    cum_column = jnp.sum(
        jnp.where(causal, jnp.broadcast_to(fall_each, (T, T)), 0.0), axis=1, keepdims=True
    )
    cum_row = jnp.sum(
        jnp.where(rows <= lanes, jnp.broadcast_to(fall_column, (T, T)), 0.0), axis=0, keepdims=True
    )
    fall = jnp.broadcast_to(jnp.sum(fall_each, axis=1, keepdims=True), (1, T))
    log_weight = jnp.broadcast_to(fall - cum_column + in_column, (T, T))
    top = jnp.max(log_weight, axis=0, keepdims=True)
    weighted = jnp.exp(log_weight - top) * (T**-0.5) * k_ref[...].astype(F32)
    memory = lax.dot_general(
        weighted.astype(BF16), v_ref[...], (((0,), (0,)), ((), ())), preferred_element_type=F32
    )
    slice_rows = T // ny
    sub8 = lax.broadcasted_iota(jnp.int32, (8, T), 0)
    for j in range(ny):
        m_send[j, 0:slice_rows] = memory[j * slice_rows : (j + 1) * slice_rows]
        m_send[j, slice_rows : slice_rows + 8] = jnp.where(
            sub8 == 0, top, jnp.where(sub8 == 1, fall, 0.0)
        )
    m_got[y] = m_send[y]

    shard = gate_w_ref.shape[0]
    lane = lax.broadcasted_iota(jnp.int32, (shard, T), 1)
    ends = []
    for n, ref in enumerate((gate_w_ref, up_w_ref, down_w_ref)):
        tail[n] = jnp.zeros((shard, T), F32)
        tail[n, :, 0:64] = ref[:, 640:704].astype(F32)
        ends.append((ref[:, 512:640].astype(F32), tail[n]))

    def rest_of(n, j, at):
        wide, narrow = ends[n]
        wide = pltpu.roll(wide, (at - 32 * j) % T, 1)
        narrow = pltpu.roll(narrow, (at + 32 - 16 * j) % T, 1)
        here = (lane >= at) & (lane < at + 48)
        return jnp.where(here, jnp.where(lane < at + 32, wide, narrow), 0.0)

    for j in range(ny):
        gu_pack[j, :, 0:128] = gate_w_ref[:, j * T : (j + 1) * T]
        gu_pack[j, :, 128:256] = up_w_ref[:, j * T : (j + 1) * T]
        gu_pack[j, :, 256:384] = (rest_of(0, j, 0) + rest_of(1, j, 64)).astype(BF16)
        d_pack[j, :, 0:128] = down_w_ref[:, j * T : (j + 1) * T]
        d_pack[j, :, 128:256] = rest_of(2, j, 0).astype(BF16)

    def gu_rows(slot, begin, count):
        return w_gu.at[slot, pl.ds(pl.multiple_of(begin, 32), count), :]

    w_gu[z, pl.ds(pl.multiple_of(y * shard, 32), shard), :] = gu_pack[y]
    d_block[pl.ds(pl.multiple_of(y * shard, 32), shard), :] = d_pack[y]
    for s in range(nz):
        w_d[s, UNITS:256] = jnp.zeros((256 - UNITS, T), BF16)
    for s in range(nz // 2):
        w_d2[s, UNITS:256] = jnp.zeros((256 - UNITS, T), BF16)

    pl.semaphore_wait(barrier, nz - 1 + 2 * nx * ny - 1)

    def send(*args, **where):
        remote(*args, **where).start()

    for dy in range(1, ny):
        to = lax.rem(y + dy, ny)
        send(m_send.at[to], m_got.at[y], ya_s.at[0], ya_r.at[0], y=to)
    for dy in range(1, ny):
        to = lax.rem(y + dy, ny)
        send(gu_pack.at[to], gu_rows(z, y * shard, shard), ya_s.at[1], ya_r.at[1], y=to)
        d_rows = pl.ds(pl.multiple_of(y * shard, 32), shard)
        send(d_pack.at[to], d_block.at[d_rows], ya_s.at[2], ya_r.at[2], y=to)

    scores = lax.dot_general(
        q_ref[...], k_ref[...], (((1,), (1,)), ((), ())), preferred_element_type=F32
    ) * (T**-0.5)

    arrived(m_got.at[0 : ny - 1], ya_s.at[0], ya_r.at[0])
    state = (jnp.zeros((slice_rows, T), F32), jnp.full((1, T), FAR, F32), jnp.zeros((1, T), F32))
    before = []
    for j in range(ny):
        before.append(state)
        got = m_got[j]
        late = (
            got[0:slice_rows],
            got[slice_rows : slice_rows + 1],
            got[slice_rows + 1 : slice_rows + 2],
        )
        state = merge(state, late)
    plane_memory, plane_top, plane_fall = state

    def packed(memory, top, fall):
        numbers = jnp.zeros((8, T), F32)
        for n, piece in enumerate((*three_pieces(top), *three_pieces(fall))):
            numbers = jnp.where(sub8 == n, piece, numbers)
        return jnp.concatenate([memory, numbers], axis=0).astype(BF16)

    section, place = z // SECTION, lax.rem(z, SECTION)
    z_send[...] = packed(plane_memory, plane_top, plane_fall)

    def plane_part(dz):
        return remote(z_send, z_got.at[dz], z_s.at[dz], z_r.at[dz], z=z + dz)

    def section_part(dz):
        return remote(s_send, s_got.at[section], s_s.at[dz], s_r.at[section], z=z + dz)

    def to_planes(act):
        for dz in range(SECTION - 1, 0, -1):
            pl.when(place + dz < SECTION)(functools.partial(act, plane_part(dz)))

    def to_sections(act):
        for dz in range(nz - SECTION, 0, -1):
            due = (place == SECTION - 1) & (z + dz < nz)
            pl.when(due)(functools.partial(act, section_part(dz)))

    to_planes(lambda copy: copy.start())

    up_z, down_z = lax.rem(z + 1, nz), lax.rem(z + nz - 1, nz)
    rounds = RING_ROUNDS

    def ring_part(way, r, m, arriving):
        step = r if arriving else r - 1
        slot = lax.rem(z + step, nz) if way else lax.rem(z + nz - step, nz)
        ref = w_d.at[slot, pl.ds(0, UNITS)] if m == 2 else gu_rows(slot, m * (T // 2), T // 2)
        to = down_z if way else up_z
        return remote(ref, ref, ring_s.at[2 * way + m // 2], ring_r.at[way, m, r], z=to)

    def lend(slot):
        @pl.when(lax.rem(slot // 2, 2) == other)
        def _():
            there = w_d2.at[2 * (slot // 4) + lax.rem(slot, 2), pl.ds(0, UNITS)]
            send(w_d.at[slot, pl.ds(0, UNITS)], there, d2_s, d2_r, c=other)

    def ring_begin(way):
        for m in range(3):
            ring_part(way, 1, m, False).start()

    turns = [[(r, m) for r in range(1, rounds[way] + 1) for m in range(3)] for way in range(2)]

    def ring_turns(way, count):
        for r, m in turns[way][:count]:
            ring_part(way, r, m, True).wait_recv()
            if r < rounds[way]:
                ring_part(way, r + 1, m, False).start()
            if m == 2:
                lend(lax.rem(z + r, nz) if way else lax.rem(z + nz - r, nz))
        del turns[way][:count]

    def both_turns(up, down):
        for n in range(max(up, down)):
            if n < up:
                ring_turns(0, 1)
            if n < down:
                ring_turns(1, 1)

    arrived(gu_pack.at[0 : ny - 1], ya_s.at[1], ya_r.at[1])
    arrived(d_pack.at[0 : ny - 1], ya_s.at[2], ya_r.at[2])
    turned = jnp.transpose(d_block[...].astype(F32))
    w_d[z, 0:UNITS] = turned[0:UNITS].astype(BF16)

    def passing(carry, got):
        total, highest, fallen = carry
        got = got.astype(F32)
        found = got[slice_rows : slice_rows + 8]
        level = found[0:1] + found[1:2] + found[2:3] + fallen
        new = jnp.maximum(highest, level)
        total = total * jnp.exp(highest - new) + jnp.exp(level - new) * got[0:slice_rows]
        return total, new, fallen + (found[3:4] + found[4:5] + found[5:6])

    def pass_plane(dz, carry):
        arrived(z_got.at[dz], z_s.at[dz], z_r.at[dz])
        return passing(carry, z_got[dz])

    def pass_section(n, carry):
        n = section - 1 - n
        arrived(s_got.at[n], s_s.at[0], s_r.at[n])
        return passing(carry, s_got[n])

    ring_begin(0)
    ring_begin(1)
    lend(z)
    both_turns(*TURNS[0])
    passed = (jnp.zeros((slice_rows, T), F32), jnp.full((1, T), FAR, F32), jnp.zeros((1, T), F32))
    passed = lax.fori_loop(1, place + 1, pass_plane, passed)
    s_send[...] = packed(*merge(passed, (plane_memory, plane_top, plane_fall)))
    to_sections(lambda copy: copy.start())
    both_turns(*TURNS[1])
    total, highest, fallen = lax.fori_loop(0, section, pass_section, passed)
    top_in = jnp.maximum(fallen, highest)
    plane_in = (total * jnp.exp(highest - top_in), top_in, jnp.zeros((1, T), F32))
    for j in range(ny):
        memory_j, top_j, _ = merge(plane_in, before[j])
        e_send[j, 0:slice_rows] = memory_j
        e_send[j, slice_rows : slice_rows + 8] = jnp.broadcast_to(top_j, (8, T))
    e_got[y] = e_send[y]
    for dy in range(1, ny):
        to = lax.rem(y + dy, ny)
        send(e_send.at[to], e_got.at[y], e_s, e_r, y=to)
    both_turns(*TURNS[2])
    arrived(e_got.at[0 : ny - 1], e_s, e_r)

    memory_in = jnp.concatenate([e_got[j, 0:slice_rows] for j in range(ny)], axis=0)
    top_here = e_got[0, slice_rows : slice_rows + 1]
    cum_wide = jnp.broadcast_to(cum_column, (T, T))
    carried = cum_wide + top_here
    spread = jnp.where(causal, cum_wide - cum_row + in_row, -jnp.inf)
    row_top = jnp.maximum(carried, jnp.max(spread, axis=1, keepdims=True))
    block_weights = (scores * jnp.exp(spread - row_top)).astype(BF16)
    inner = dot(block_weights, v_ref[...])
    outer = sum(dot(q_ref[...], piece.astype(BF16)) for piece in three_pieces(memory_in))
    readout = jnp.exp(carried - row_top) * outer + inner
    scale = lax.rsqrt(jnp.mean(readout * readout, axis=1, keepdims=True) + EPS)
    normed_heads = (readout * scale * head_gain_ref[pl.ds(tp, 1), :]).astype(BF16)
    heads[tp] = normed_heads
    for d in range(1, n_tp):
        to = lax.rem(tp + d, n_tp)
        send(heads.at[tp], heads.at[tp], h_s, h_r, x=to // 2, c=to % 2)

    both_turns(*TURNS[3])

    arrived(heads.at[0 : n_tp - 1], h_s, h_r)
    mixed = stream_ref[...].astype(F32)
    for n in range(nx):
        pair = jnp.concatenate([heads[2 * n], heads[2 * n + 1]], axis=1)
        mixed = mixed + dot(pair, out_w_ref[n * WIDE : (n + 1) * WIDE, :])
    mixed_ref[...] = mixed
    own_tokens = pl.ds(pl.multiple_of(y * T, T), T)
    for half in range(2):
        gain = norm_gain_ref[pl.ds(2 * tp + half, 1), :]
        part = mixed[:, half * T : (half + 1) * T]
        acts[tp, own_tokens, half * T : (half + 1) * T] = (part * gain).astype(BF16)
    square_column = jnp.sum(mixed * mixed, axis=1, keepdims=True)
    square_row = jnp.sum(
        jnp.where(same, jnp.broadcast_to(square_column, (T, T)), 0.0), axis=0, keepdims=True
    )
    squares[tp * ny + y] = jnp.broadcast_to(square_row, (8, T))

    def piece_of(tp_there, y_there):
        tokens = pl.ds(pl.multiple_of(y_there * T, T), T)
        return acts.at[tp_there, tokens, :], squares.at[tp_there * ny + y_there]

    def pass_on(dy, dxs):
        for dx in dxs:
            tp_there = lax.rem(x + nx - dx, nx) * 2 + c
            for m, ref in enumerate(piece_of(tp_there, lax.rem(y + ny - dy, ny))):
                send(ref, ref, p_s.at[m], p_r.at[m, dy], c=other)

    for dy in GROUPS:
        for dx in GROUPS:
            if dx or dy:
                for m, ref in enumerate(piece_of(tp, y)):
                    there = dict(x=lax.rem(x + dx, nx), y=lax.rem(y + dy, ny))
                    send(ref, ref, a_s.at[m], a_r.at[m, dy], **there)
    pass_on(0, (0,))

    both_turns(len(turns[0]), len(turns[1]))
    for dy in GROUPS:
        dxs = [dx for dx in GROUPS if dx or dy]
        arrived(r_got.at[0 : len(dxs)], a_s.at[0], a_r.at[0, dy])
        arrived(squares.at[0 : len(dxs)], a_s.at[1], a_r.at[1, dy])
        pass_on(dy, dxs)

    lane_wide = lax.broadcasted_iota(jnp.int32, (T, T), 1)

    def tokens_of(dy):
        return pl.ds(pl.multiple_of(lax.rem(y + ny - dy, ny) * T, T), T)

    def make_hidden(n):
        dy = GROUPS[n]
        arrived(r_got.at[0:nx], p_s.at[0], p_r.at[0, dy])
        arrived(squares.at[0:nx], p_s.at[1], p_r.at[1, dy])
        tokens = tokens_of(dy)
        total_square = jnp.zeros((1, T), F32)
        both = jnp.zeros((T, 3 * T), F32)
        for b in range(n_tp):
            total_square = total_square + squares[b * ny + lax.rem(y + ny - dy, ny)][0:1]
            both = both + dot(acts[b, tokens, :], w_gu[2 * b : 2 * b + 2].reshape(2 * T, 3 * T))
        factor = lax.rsqrt(column(total_square) * (1.0 / (n_tp * WIDE)) + EPS)
        both = both * factor
        gate, up, rest = both[:, 0:T], both[:, T : 2 * T], both[:, 2 * T : 3 * T]
        here = slice(n * T, (n + 1) * T)
        hidden[c, here, 0:T] = (gate / (1.0 + jnp.exp(-gate)) * up).astype(BF16)
        small = rest / (1.0 + jnp.exp(-rest)) * pltpu.roll(rest, 64, 1)
        hidden[c, here, T : 2 * T] = jnp.where(lane_wide < 48, small, 0.0).astype(BF16)
        ref = hidden.at[c, here, :]
        send(ref, ref, x_s, x_r.at[n], c=other)

    def share_out(first, last):
        for n in range(first, last):
            arrived(hidden.at[other, n * T : (n + 1) * T, :], x_s, x_r.at[n])
        mine, partners = (hidden[core, first * T : last * T, :] for core in (c, other))
        for dx in GROUPS:
            b = lax.rem(x + nx - dx, nx)
            own = jnp.concatenate([w_d[4 * b + 2 * c], w_d[4 * b + 2 * c + 1]], axis=1)
            theirs = jnp.concatenate([w_d2[2 * b], w_d2[2 * b + 1]], axis=1)
            share = (dot(mine, own) + dot(partners, theirs)).astype(BF16)
            for n in range(first, last):
                dy = GROUPS[n]
                to = dx * ny + dy
                r_send[to] = share[(n - first) * T : (n - first + 1) * T]
                if to:
                    there = dict(x=b, y=lax.rem(y + ny - dy, ny))
                    send(r_send.at[to], r_got.at[to], r_s, r_r.at[dy], **there)

    make_hidden(0)
    make_hidden(1)
    arrived(w_d2.at[0 : 2 * nx, pl.ds(0, UNITS)], d2_s, d2_r)
    share_out(0, 1)
    make_hidden(2)
    make_hidden(3)
    share_out(1, 4)
    channel = r_send[0].astype(F32)
    for dy in GROUPS:
        dxs = [dx for dx in GROUPS if dx or dy]
        arrived(r_got.at[0 : len(dxs)], r_s, r_r.at[dy])
        for dx in dxs:
            channel = channel + r_got[dx * ny + dy].astype(F32)
    out_ref[...] = mixed_ref[...] + 0.5 * channel

    to_planes(lambda copy: copy.wait_send())
    to_sections(lambda copy: copy.wait_send())

    def gone(ref, sem):
        remote(ref, ref, sem, x_r.at[0], c=other).wait_send()

    gone(m_send.at[0 : ny - 1], ya_s.at[0])
    gone(gu_pack.at[0 : ny - 1], ya_s.at[1])
    gone(d_pack.at[0 : ny - 1], ya_s.at[2])
    gone(e_send.at[0 : ny - 1], e_s)
    gone(heads.at[0 : n_tp - 1], h_s)
    for way in range(2):
        gone(w_gu.at[0 : rounds[way]], ring_s.at[2 * way])
        gone(w_d.at[0 : rounds[way], pl.ds(0, UNITS)], ring_s.at[2 * way + 1])
    gone(r_got.at[0 : nx * ny - 1], a_s.at[0])
    gone(squares.at[0 : nx * ny - 1], a_s.at[1])
    gone(r_got.at[0 : nx * ny], p_s.at[0])
    gone(squares.at[0 : nx * ny], p_s.at[1])
    gone(w_d.at[0 : 2 * nx, pl.ds(0, UNITS)], d2_s)
    gone(hidden.at[0], x_s)
    gone(r_got.at[0 : nx * ny - 1], r_s)


def local(nz, ny, nx, *args):
    queries, keys, values, in_gate, forget_gate, stream = args[:6]
    head_gain, out_weight, norm_gain, gate_weight, up_weight, down_weight = args[6:]
    n_tp = 2 * nx
    dma = pltpu.SemaphoreType.DMA
    vmem = pltpu.VMEM
    slice_rows = T // ny
    shard = gate_weight.shape[0]
    scratch = [
        vmem((3, shard, T), F32),
        vmem((ny, shard, 3 * T), BF16),
        vmem((ny, shard, 2 * T), BF16),
        vmem((T, 2 * T), BF16),
        vmem((nz, T, 3 * T), BF16),
        vmem((nz, 256, T), BF16),
        vmem((nz // 2, 256, T), BF16),
        vmem((ny, slice_rows + 8, T), F32),
        vmem((ny, slice_rows + 8, T), F32),
        vmem((slice_rows + 8, T), BF16),
        vmem((SECTION, slice_rows + 8, T), BF16),
        vmem((slice_rows + 8, T), BF16),
        vmem((nz // SECTION, slice_rows + 8, T), BF16),
        vmem((ny, slice_rows + 8, T), F32),
        vmem((ny, slice_rows + 8, T), F32),
        vmem((n_tp, T, T), BF16),
        vmem((T, WIDE), F32),
        vmem((n_tp, ny * T, WIDE), BF16),
        vmem((n_tp * ny, 8, T), F32),
        vmem((2, ny * T, 2 * T), BF16),
        vmem((nx * ny, T, WIDE), BF16),
        vmem((nx * ny, T, WIDE), BF16),
        dma((3,)),
        dma((3,)),
        dma((SECTION,)),
        dma((SECTION,)),
        dma((nz - SECTION + 1,)),
        dma((nz // SECTION,)),
        dma,
        dma,
        dma((4,)),
        dma((2, 3, max(RING_ROUNDS) + 1)),
        dma,
        dma,
        dma((2,)),
        dma((2, ny)),
        dma((2,)),
        dma((2, ny)),
        dma,
        dma,
        dma,
        dma((ny,)),
        dma,
        dma((ny,)),
    ]
    return pl.pallas_call(
        functools.partial(kernel, nz, ny, nx),
        out_shape=jax.ShapeDtypeStruct((T, WIDE), F32),
        in_specs=[pl.BlockSpec(memory_space=vmem)] * 12,
        out_specs=pl.BlockSpec(memory_space=vmem),
        scratch_shapes=scratch,
        compiler_params=pltpu.CompilerParams(collective_id=0, has_side_effects=True),
        name="layer",
    )(
        queries,
        keys,
        values,
        in_gate,
        forget_gate,
        stream,
        head_gain.reshape(n_tp, T),
        out_weight,
        norm_gain.reshape(2 * n_tp, T),
        gate_weight,
        up_weight,
        down_weight,
    )


def solution(mesh):
    nz, ny, nx = 16, 4, mesh.shape["tp"] // 2
    finer = Mesh(mesh.devices.reshape(nz, ny, nx, 2), ("z", "y", "x", "c"))
    rows, columns = ("z", "y"), ("x", "c")
    in_specs = (
        P(rows, columns),
        P(rows, columns),
        P(rows, columns),
        P(columns, rows),
        P(columns, rows),
        P(rows, columns),
        P(),
        P(None, columns),
        P(),
        P(rows, columns),
        P(rows, columns),
        P(rows, columns),
    )
    return jax.shard_map(
        functools.partial(local, nz, ny, nx),
        mesh=finer,
        in_specs=in_specs,
        out_specs=P(rows, columns),
        check_vma=False,
    )
```

time: 97.5 us -> 80.5 us (0.83)
  Pallas kernels: 95.8 us -> 78.8 us
    pallas_call x1, Pallas kernels: 95.8 us -> 78.8 us  [local(): pl.pallas_call(functools.partial(kernel, nz, ny, nx), out_shape=jax.Shape...]
where the time goes in v2:
time: 80.5 us; the launch traced here: 80.4 us
  Pallas kernels  78.8 us (98%)
  local copies, waits for them, and re-layouts  1.57 us (2%)
    pallas_call x1, Pallas kernels, local(): pl.pallas_call(functools.partial(kernel, nz, ny, nx), out_shape=jax.Shape...  78.8 us

profile of v2, /device:TPU:1, one launch (start us, length us, event | category | flops | bytes accessed | tf_op | source)
XLA Modules:
  0.0 80.4 jit_solution(5256773483987198245)
XLA Ops:
  0.0 78.8 %layer.1 = f32[128,256]{1,0:T(8,128)} custom-call(bf16[128,128]{1,0:T(8,128)(2,1)} %q_ref.1, bf16[128,128]{1,0:T(8,128)(2,1)} %k_ref.1, bf16[128,128]{1,0:T(8,128)(2,1)} %v_ref.1, f32[1,128]{1,0:T(1,128)} %in_ref.1, f32[1,128]{1,0:T(1,128)} %forget_ref.1, bf16[128,256]{1,0:T(8,128)(2,1)} %stream_ref.1, f32[8,128]{1,0:T(8,128)} %bitcast.3, ...), custom_call_target="tpu_custom_call" | custom-call | tf_op jit(solution)/shard_map/layer/pallas_call | solution.py:542
  78.8 1.6 %copy.14 = f32[128,256]{1,0:T(8,128)} copy(f32[128,256]{1,0:T(8,128)} %layer.1) | data formatting | bytes 262144

commit v3 on v2

--- a/solution.py
+++ b/solution.py
@@ -18,8 +18,9 @@
 EPS = 1e-6
 FAR = -1e30
 SECTION = 4
-TURNS = ((1, 1), (6, 6), (3, 3), (3, 3))
-GROUPS = (2, 1, 3, 0)
+TURNS = ((0, 0), (6, 6), (3, 3), (5, 5), (4, 4))
+FIRST = 3
+GROUPS = (0, 3, 2, 1)
 RING_ROUNDS = (8, 7)
 
 
@@ -46,6 +47,19 @@
     nz,
     ny,
     nx,
+    q_hbm,
+    k_hbm,
+    v_hbm,
+    in_hbm,
+    forget_hbm,
+    stream_hbm,
+    head_gain_hbm,
+    out_w_hbm,
+    norm_gain_hbm,
+    gate_w_hbm,
+    up_w_hbm,
+    down_w_hbm,
+    out_ref,
     q_ref,
     k_ref,
     v_ref,
@@ -58,7 +72,7 @@
     gate_w_ref,
     up_w_ref,
     down_w_ref,
-    out_ref,
+    load_s,
     tail,
     gu_pack,
     d_pack,
@@ -79,8 +93,15 @@
     acts,
     squares,
     hidden,
-    r_send,
-    r_got,
+    ra_send,
+    ra_got,
+    rb_send,
+    rb_got,
+    sa_send,
+    sa_got,
+    sb_send,
+    sb_got,
+    entered,
     ya_s,
     ya_r,
     z_s,
@@ -94,15 +115,30 @@
     h_s,
     h_r,
     a_s,
-    a_r,
+    ax_r,
+    ay_r,
+    as_s,
+    asx_r,
+    asy_r,
+    f_s,
+    f_s2,
+    fa_r,
+    fb_r,
     p_s,
     p_r,
+    ps_r,
     d2_s,
     d2_r,
     x_s,
     x_r,
     r_s,
-    r_r,
+    rb_s,
+    ra_r,
+    rb_r,
+    s2_s,
+    s3_s,
+    sa_r,
+    sb_r,
 ):
     z, y, x, c = (lax.axis_index(a) for a in ("z", "y", "x", "c"))
     tp = x * 2 + c
@@ -128,13 +164,35 @@
         pl.semaphore_signal(barrier, inc=1, device_id=where, device_id_type=MESH)
 
     for dz in range(1, nz):
-        greet(z=lax.rem(z + dz, nz))
+        pl.when(z + dz < nz)(functools.partial(greet, z=z + dz))
     plane = [(dx, dy) for dx in range(nx) for dy in range(ny)]
     for dx, dy in plane:
         for dc in range(2):
             if dx or dy or dc:
                 greet(x=lax.rem(x + dx, nx), y=lax.rem(y + dy, ny), c=lax.rem(c + dc, 2))
 
+    pairs = (
+        (in_hbm, in_ref),
+        (forget_hbm, forget_ref),
+        (k_hbm, k_ref),
+        (v_hbm, v_ref),
+        (gate_w_hbm, gate_w_ref),
+        (up_w_hbm, up_w_ref),
+        (down_w_hbm, down_w_ref),
+        (q_hbm, q_ref),
+        (stream_hbm, stream_ref),
+        (head_gain_hbm, head_gain_ref),
+        (norm_gain_hbm, norm_gain_ref),
+        (out_w_hbm, out_w_ref),
+    )
+    loads = [
+        pltpu.make_async_copy(hbm, ref, load_s.at[n]) for n, (hbm, ref) in enumerate(pairs)
+    ]
+    for copy in loads:
+        copy.start()
+
+    for copy in loads[0:4]:
+        copy.wait()
     rows = lax.broadcasted_iota(jnp.int32, (T, T), 0)
     lanes = lax.broadcasted_iota(jnp.int32, (T, T), 1)
     causal = rows >= lanes
@@ -170,6 +228,8 @@
         )
     m_got[y] = m_send[y]
 
+    for copy in loads[4:7]:
+        copy.wait()
     shard = gate_w_ref.shape[0]
     lane = lax.broadcasted_iota(jnp.int32, (shard, T), 1)
     ends = []
@@ -202,7 +262,20 @@
     for s in range(nz // 2):
         w_d2[s, UNITS:256] = jnp.zeros((256 - UNITS, T), BF16)
 
-    pl.semaphore_wait(barrier, nz - 1 + 2 * nx * ny - 1)
+    pl.semaphore_wait(barrier, 2 * nx * ny - 1 + z)
+    section, place = z // SECTION, lax.rem(z, SECTION)
+    for dz in range(1, nz):
+        from_last = lax.rem(z + nz - dz, SECTION) == SECTION - 1
+        awaited = from_last | (place >= dz) if dz < SECTION else from_last
+        if dz == 1 or dz == nz - 1:
+            awaited = True
+        answer = functools.partial(
+            pl.semaphore_signal, entered.at[dz], inc=1, device_id_type=MESH
+        )
+        pl.when((z >= dz) & awaited)(functools.partial(answer, device_id=dict(z=z - dz)))
+
+    def is_in(dz):
+        pl.semaphore_wait(entered.at[dz], 1)
 
     def send(*args, **where):
         remote(*args, **where).start()
@@ -216,6 +289,8 @@
         d_rows = pl.ds(pl.multiple_of(y * shard, 32), shard)
         send(d_pack.at[to], d_block.at[d_rows], ya_s.at[2], ya_r.at[2], y=to)
 
+    for copy in loads[7:]:
+        copy.wait()
     scores = lax.dot_general(
         q_ref[...], k_ref[...], (((1,), (1,)), ((), ())), preferred_element_type=F32
     ) * (T**-0.5)
@@ -240,7 +315,6 @@
             numbers = jnp.where(sub8 == n, piece, numbers)
         return jnp.concatenate([memory, numbers], axis=0).astype(BF16)
 
-    section, place = z // SECTION, lax.rem(z, SECTION)
     z_send[...] = packed(plane_memory, plane_top, plane_fall)
 
     def plane_part(dz):
@@ -258,6 +332,8 @@
             due = (place == SECTION - 1) & (z + dz < nz)
             pl.when(due)(functools.partial(act, section_part(dz)))
 
+    for dz in range(1, SECTION):
+        pl.when(place + dz < SECTION)(functools.partial(is_in, dz))
     to_planes(lambda copy: copy.start())
 
     up_z, down_z = lax.rem(z + 1, nz), lax.rem(z + nz - 1, nz)
@@ -280,23 +356,50 @@
         for m in range(3):
             ring_part(way, 1, m, False).start()
 
-    turns = [[(r, m) for r in range(1, rounds[way] + 1) for m in range(3)] for way in range(2)]
-
-    def ring_turns(way, count):
-        for r, m in turns[way][:count]:
-            ring_part(way, r, m, True).wait_recv()
-            if r < rounds[way]:
-                ring_part(way, r + 1, m, False).start()
-            if m == 2:
-                lend(lax.rem(z + r, nz) if way else lax.rem(z + nz - r, nz))
-        del turns[way][:count]
-
-    def both_turns(up, down):
-        for n in range(max(up, down)):
-            if n < up:
-                ring_turns(0, 1)
-            if n < down:
-                ring_turns(1, 1)
+    turns = [[(way, r, m) for r in range(1, rounds[way] + 1) for m in range(3)] for way in range(2)]
+
+    def turn(way, r, m):
+        ring_part(way, r, m, True).wait_recv()
+        if r < rounds[way]:
+            ring_part(way, r + 1, m, False).start()
+        if m == 2:
+            lend(lax.rem(z + r, nz) if way else lax.rem(z + nz - r, nz))
+
+    def all_of(up, down):
+        for n in range(max(len(up), len(down))):
+            for n in [*up[n : n + 1], *down[n : n + 1]]:
+                turn(*n)
+
+    put_off = [[], []]
+
+    def both_turns(stop):
+        here = [turns[way][: TURNS[stop][way]] for way in range(2)]
+        for way in range(2):
+            del turns[way][: TURNS[stop][way]]
+            put_off[way] += here[way]
+
+        @pl.when(z >= FIRST)
+        def _():
+            all_of(*here)
+
+    def put_off_turns(up, down):
+        here = put_off[0][:up], put_off[1][:down]
+        del put_off[0][:up], put_off[1][:down]
+
+        @pl.when(z < FIRST)
+        def _():
+            all_of(*here)
+
+    def rest_of_turns():
+        @pl.when(z >= FIRST)
+        def _():
+            all_of(*turns)
+
+        put_off_turns(*(len(p) for p in put_off))
+
+        @pl.when(z < FIRST)
+        def _():
+            all_of(*turns)
 
     arrived(gu_pack.at[0 : ny - 1], ya_s.at[1], ya_r.at[1])
     arrived(d_pack.at[0 : ny - 1], ya_s.at[2], ya_r.at[2])
@@ -321,15 +424,20 @@
         arrived(s_got.at[n], s_s.at[0], s_r.at[n])
         return passing(carry, s_got[n])
 
+    pl.when((place == SECTION - 1) & (z + 1 < nz))(functools.partial(is_in, 1))
     ring_begin(0)
+    pl.when(z == 0)(functools.partial(is_in, nz - 1))
     ring_begin(1)
     lend(z)
-    both_turns(*TURNS[0])
+    both_turns(0)
     passed = (jnp.zeros((slice_rows, T), F32), jnp.full((1, T), FAR, F32), jnp.zeros((1, T), F32))
     passed = lax.fori_loop(1, place + 1, pass_plane, passed)
     s_send[...] = packed(*merge(passed, (plane_memory, plane_top, plane_fall)))
+    for dz in range(2, nz - SECTION + 1):
+        due = (place == SECTION - 1) & (z + dz < nz)
+        pl.when(due)(functools.partial(is_in, dz))
     to_sections(lambda copy: copy.start())
-    both_turns(*TURNS[1])
+    both_turns(1)
     total, highest, fallen = lax.fori_loop(0, section, pass_section, passed)
     top_in = jnp.maximum(fallen, highest)
     plane_in = (total * jnp.exp(highest - top_in), top_in, jnp.zeros((1, T), F32))
@@ -341,7 +449,7 @@
     for dy in range(1, ny):
         to = lax.rem(y + dy, ny)
         send(e_send.at[to], e_got.at[y], e_s, e_r, y=to)
-    both_turns(*TURNS[2])
+    both_turns(2)
     arrived(e_got.at[0 : ny - 1], e_s, e_r)
 
     memory_in = jnp.concatenate([e_got[j, 0:slice_rows] for j in range(ny)], axis=0)
@@ -361,7 +469,8 @@
         to = lax.rem(tp + d, n_tp)
         send(heads.at[tp], heads.at[tp], h_s, h_r, x=to // 2, c=to % 2)
 
-    both_turns(*TURNS[3])
+    both_turns(3)
+    put_off_turns(4, 4)
 
     arrived(heads.at[0 : n_tp - 1], h_s, h_r)
     mixed = stream_ref[...].astype(F32)
@@ -380,31 +489,67 @@
     )
     squares[tp * ny + y] = jnp.broadcast_to(square_row, (8, T))
 
-    def piece_of(tp_there, y_there):
-        tokens = pl.ds(pl.multiple_of(y_there * T, T), T)
-        return acts.at[tp_there, tokens, :], squares.at[tp_there * ny + y_there]
-
-    def pass_on(dy, dxs):
-        for dx in dxs:
-            tp_there = lax.rem(x + nx - dx, nx) * 2 + c
-            for m, ref in enumerate(piece_of(tp_there, lax.rem(y + ny - dy, ny))):
-                send(ref, ref, p_s.at[m], p_r.at[m, dy], c=other)
-
-    for dy in GROUPS:
-        for dx in GROUPS:
-            if dx or dy:
-                for m, ref in enumerate(piece_of(tp, y)):
-                    there = dict(x=lax.rem(x + dx, nx), y=lax.rem(y + dy, ny))
-                    send(ref, ref, a_s.at[m], a_r.at[m, dy], **there)
-    pass_on(0, (0,))
-
-    both_turns(len(turns[0]), len(turns[1]))
-    for dy in GROUPS:
-        dxs = [dx for dx in GROUPS if dx or dy]
-        arrived(r_got.at[0 : len(dxs)], a_s.at[0], a_r.at[0, dy])
-        arrived(squares.at[0 : len(dxs)], a_s.at[1], a_r.at[1, dy])
-        pass_on(dy, dxs)
-
+    def part_of(dx, dy, lanes, core):
+        tokens = pl.ds(pl.multiple_of(lax.rem(y + ny - dy, ny) * T, T), T)
+        return acts.at[lax.rem(x + nx - dx, nx) * 2 + core, tokens, lanes]
+
+    def square_of(dx, dy):
+        return squares.at[
+            (lax.rem(x + nx - dx, nx) * 2 + c) * ny + lax.rem(y + ny - dy, ny)
+        ]
+
+    def to_partner(dx, dy, lanes, n, with_square=True):
+        ref = part_of(dx, dy, lanes, c)
+        send(ref, ref, p_s.at[0], p_r.at[n], c=other)
+        if with_square:
+            ref = square_of(dx, dy)
+            send(ref, ref, p_s.at[1], ps_r.at[min(dy, 1)], c=other)
+
+    ALL, LOW, HIGH = pl.ds(0, WIDE), pl.ds(0, T), pl.ds(T, T)
+    own, own_square = part_of(0, 0, ALL, c), square_of(0, 0)
+    for d in (2, 1, 3):
+        there = dict(x=lax.rem(x + d, nx))
+        send(own, own, a_s, ax_r.at[d], **there)
+        send(own_square, own_square, as_s, asx_r, **there)
+        there = dict(y=lax.rem(y + d, ny))
+        send(own, own, a_s, ay_r.at[d], **there)
+        send(own_square, own_square, as_s, asy_r, **there)
+    to_partner(0, 0, ALL, 0)
+
+    both_turns(4)
+    put_off_turns(5, 5)
+    arrived(squares.at[0:3], as_s, asx_r)
+    for e in (1, 3, 2):
+        arrived(ra_got.at[0:2], a_s, ax_r.at[e])
+        for d in (2, 1, 3):
+            there = dict(y=lax.rem(y + d, ny))
+            ref = part_of(e, 0, LOW, c)
+            send(ref, ref, f_s, fa_r, **there)
+            ref = square_of(e, 0)
+            send(ref, ref, as_s, asy_r, **there)
+        arrived(ra_got.at[0:2], a_s, ay_r.at[e])
+        for d in (2, 1, 3):
+            ref = part_of(0, e, HIGH, c)
+            send(ref, ref, f_s2, fb_r, x=lax.rem(x + d, nx))
+        to_partner(e, 0, ALL, 0)
+        to_partner(0, e, ALL, 1, False)
+    def corners_on():
+        corners = [(dx, dy) for dx in (1, 2, 3) for dy in (1, 2, 3)]
+        arrived(ra_got.at[0:9], f_s, fa_r)
+        for dx, dy in corners:
+            to_partner(dx, dy, LOW, 2, False)
+        arrived(squares.at[0:12], as_s, asy_r)
+        for dx in range(nx):
+            for dy in (1, 2, 3):
+                ref = square_of(dx, dy)
+                send(ref, ref, p_s.at[1], ps_r.at[1], c=other)
+        arrived(ra_got.at[0:9], f_s, fb_r)
+        for dx, dy in corners:
+            to_partner(dx, dy, HIGH, 3, False)
+
+    put_off_turns(7, 7)
+    pl.when(z < FIRST)(corners_on)
+    rest_of_turns()
     lane_wide = lax.broadcasted_iota(jnp.int32, (T, T), 1)
 
     def tokens_of(dy):
@@ -412,8 +557,6 @@
 
     def make_hidden(n):
         dy = GROUPS[n]
-        arrived(r_got.at[0:nx], p_s.at[0], p_r.at[0, dy])
-        arrived(squares.at[0:nx], p_s.at[1], p_r.at[1, dy])
         tokens = tokens_of(dy)
         total_square = jnp.zeros((1, T), F32)
         both = jnp.zeros((T, 3 * T), F32)
@@ -430,37 +573,74 @@
         ref = hidden.at[c, here, :]
         send(ref, ref, x_s, x_r.at[n], c=other)
 
+    arrived(ra_got.at[0 : 2 * nx], p_s.at[0], p_r.at[0])
+    arrived(squares.at[0:nx], p_s.at[1], ps_r.at[0])
+    make_hidden(0)
+    pl.when(z >= FIRST)(corners_on)
+
     def share_out(first, last):
         for n in range(first, last):
             arrived(hidden.at[other, n * T : (n + 1) * T, :], x_s, x_r.at[n])
         mine, partners = (hidden[core, first * T : last * T, :] for core in (c, other))
-        for dx in GROUPS:
+        for dx in (2, 1, 3, 0):
             b = lax.rem(x + nx - dx, nx)
             own = jnp.concatenate([w_d[4 * b + 2 * c], w_d[4 * b + 2 * c + 1]], axis=1)
             theirs = jnp.concatenate([w_d2[2 * b], w_d2[2 * b + 1]], axis=1)
             share = (dot(mine, own) + dot(partners, theirs)).astype(BF16)
             for n in range(first, last):
                 dy = GROUPS[n]
-                to = dx * ny + dy
-                r_send[to] = share[(n - first) * T : (n - first + 1) * T]
-                if to:
-                    there = dict(x=b, y=lax.rem(y + ny - dy, ny))
-                    send(r_send.at[to], r_got.at[to], r_s, r_r.at[dy], **there)
-
-    make_hidden(0)
+                at = slice((n - first) * T, (n - first + 1) * T)
+                ra_send[dx * ny + dy] = share[at, 0:T]
+                rb_send[dy * nx + dx] = share[at, T : 2 * T]
+                if dx:
+                    n_a = dx * ny + dy
+                    send(ra_send.at[n_a], ra_got.at[n_a], r_s, ra_r.at[dy], x=b)
+        for n in range(first, last):
+            dy = GROUPS[n]
+            if dy:
+                block = pl.ds(dy * nx, nx)
+                there = dict(y=lax.rem(y + ny - dy, ny))
+                send(rb_send.at[block], rb_got.at[block], rb_s, rb_r, **there)
+
+    arrived(ra_got.at[0:6], p_s.at[0], p_r.at[1])
+    arrived(squares.at[0 : nx * (ny - 1)], p_s.at[1], ps_r.at[1])
+    for n in (2, 3):
+        arrived(ra_got.at[0:9], p_s.at[0], p_r.at[n])
+    make_hidden(2)
+    make_hidden(3)
     make_hidden(1)
     arrived(w_d2.at[0 : 2 * nx, pl.ds(0, UNITS)], d2_s, d2_r)
-    share_out(0, 1)
-    make_hidden(2)
-    make_hidden(3)
-    share_out(1, 4)
-    channel = r_send[0].astype(F32)
-    for dy in GROUPS:
-        dxs = [dx for dx in GROUPS if dx or dy]
-        arrived(r_got.at[0 : len(dxs)], r_s, r_r.at[dy])
-        for dx in dxs:
-            channel = channel + r_got[dx * ny + dy].astype(F32)
-    out_ref[...] = mixed_ref[...] + 0.5 * channel
+    share_out(2, 4)
+    share_out(0, 2)
+
+    def summed(first, got, places):
+        total = first.astype(F32)
+        for n in places:
+            total = total + got[n].astype(F32)
+        return total
+
+    def low_sum(dy):
+        arrived(ra_got.at[0 : nx - 1], r_s, ra_r.at[dy])
+        return summed(ra_send[dy], ra_got, [dx * ny + dy for dx in range(1, nx)])
+
+    for dy in (2, 1, 3):
+        sa_send[dy] = low_sum(dy).astype(BF16)
+        send(sa_send.at[dy], sa_got.at[dy], s2_s, sa_r, y=lax.rem(y + ny - dy, ny))
+    arrived(rb_got.at[0 : nx * (ny - 1)], r_s, rb_r)
+
+    def high_sum(dx):
+        return summed(rb_send[dx], rb_got, [dy * nx + dx for dy in range(1, ny)])
+
+    for dx in (2, 1, 3):
+        sb_send[dx] = high_sum(dx).astype(BF16)
+        send(sb_send.at[dx], sb_got.at[dx], s3_s, sb_r, x=lax.rem(x + nx - dx, nx))
+    low, high = low_sum(0), high_sum(0)
+    arrived(sa_got.at[0 : ny - 1], s2_s, sa_r)
+    low = summed(low, sa_got, range(1, ny))
+    out_ref[:, 0:T] = mixed_ref[:, 0:T] + 0.5 * low
+    arrived(sb_got.at[0 : nx - 1], s2_s, sb_r)
+    high = summed(high, sb_got, range(1, nx))
+    out_ref[:, T:WIDE] = mixed_ref[:, T:WIDE] + 0.5 * high
 
     to_planes(lambda copy: copy.wait_send())
     to_sections(lambda copy: copy.wait_send())
@@ -476,13 +656,18 @@
     for way in range(2):
         gone(w_gu.at[0 : rounds[way]], ring_s.at[2 * way])
         gone(w_d.at[0 : rounds[way], pl.ds(0, UNITS)], ring_s.at[2 * way + 1])
-    gone(r_got.at[0 : nx * ny - 1], a_s.at[0])
-    gone(squares.at[0 : nx * ny - 1], a_s.at[1])
-    gone(r_got.at[0 : nx * ny], p_s.at[0])
+    gone(ra_got.at[0:12], a_s)
+    gone(squares.at[0:15], as_s)
+    gone(ra_got.at[0:9], f_s)
+    gone(rb_got.at[0:9], f_s2)
+    gone(acts.at[0:nx], p_s.at[0])
     gone(squares.at[0 : nx * ny], p_s.at[1])
     gone(w_d.at[0 : 2 * nx, pl.ds(0, UNITS)], d2_s)
     gone(hidden.at[0], x_s)
-    gone(r_got.at[0 : nx * ny - 1], r_s)
+    gone(ra_got.at[0 : nx * ny - ny], r_s)
+    gone(rb_got.at[0 : nx * ny - nx], rb_s)
+    gone(sa_got.at[0 : ny - 1], s2_s)
+    gone(sb_got.at[0 : nx - 1], s3_s)
 
 
 def local(nz, ny, nx, *args):
@@ -493,7 +678,23 @@
     vmem = pltpu.VMEM
     slice_rows = T // ny
     shard = gate_weight.shape[0]
-    scratch = [
+    arrays = (
+        queries,
+        keys,
+        values,
+        in_gate,
+        forget_gate,
+        stream,
+        head_gain.reshape(n_tp, T),
+        out_weight,
+        norm_gain.reshape(2 * n_tp, T),
+        gate_weight,
+        up_weight,
+        down_weight,
+    )
+    scratch = [vmem(a.shape, a.dtype) for a in arrays]
+    scratch += [
+        dma((len(arrays),)),
         vmem((3, shard, T), F32),
         vmem((ny, shard, 3 * T), BF16),
         vmem((ny, shard, 2 * T), BF16),
@@ -514,8 +715,15 @@
         vmem((n_tp, ny * T, WIDE), BF16),
         vmem((n_tp * ny, 8, T), F32),
         vmem((2, ny * T, 2 * T), BF16),
-        vmem((nx * ny, T, WIDE), BF16),
-        vmem((nx * ny, T, WIDE), BF16),
+        vmem((nx * ny, T, T), BF16),
+        vmem((nx * ny, T, T), BF16),
+        vmem((nx * ny, T, T), BF16),
+        vmem((nx * ny, T, T), BF16),
+        vmem((ny, T, T), BF16),
+        vmem((ny, T, T), BF16),
+        vmem((nx, T, T), BF16),
+        vmem((nx, T, T), BF16),
+        pltpu.SemaphoreType.REGULAR((nz,)),
         dma((3,)),
         dma((3,)),
         dma((SECTION,)),
@@ -528,39 +736,41 @@
         dma((2, 3, max(RING_ROUNDS) + 1)),
         dma,
         dma,
+        dma,
+        dma((nx,)),
+        dma((ny,)),
+        dma,
+        dma,
+        dma,
+        dma,
+        dma,
+        dma,
+        dma,
         dma((2,)),
-        dma((2, ny)),
+        dma((4,)),
         dma((2,)),
-        dma((2, ny)),
         dma,
         dma,
         dma,
         dma((ny,)),
         dma,
+        dma,
         dma((ny,)),
+        dma,
+        dma,
+        dma,
+        dma,
+        dma,
     ]
     return pl.pallas_call(
         functools.partial(kernel, nz, ny, nx),
-        out_shape=jax.ShapeDtypeStruct((T, WIDE), F32),
-        in_specs=[pl.BlockSpec(memory_space=vmem)] * 12,
+        out_shape=vmem((T, WIDE), F32),
+        in_specs=[pl.BlockSpec(memory_space=pl.ANY)] * 12,
         out_specs=pl.BlockSpec(memory_space=vmem),
         scratch_shapes=scratch,
         compiler_params=pltpu.CompilerParams(collective_id=0, has_side_effects=True),
         name="layer",
-    )(
-        queries,
-        keys,
-        values,
-        in_gate,
-        forget_gate,
-        stream,
-        head_gain.reshape(n_tp, T),
-        out_weight,
-        norm_gain.reshape(2 * n_tp, T),
-        gate_weight,
-        up_weight,
-        down_weight,
-    )
+    )(*arrays)
 
 
 def solution(mesh):

time: 80.5 us -> 70.8 us (0.88)
  Pallas kernels: 78.8 us -> 70 us
  local copies, waits for them, and re-layouts: 1.57 us -> 0.66 us
    pallas_call x1, Pallas kernels: 78.8 us -> 70 us  [local(): pl.pallas_call(functools.partial(kernel, nz, ny, nx), out_shape=vmem((T,...]
    unnamed x1, local copies, waits for them, and re-layouts: 1.57 us -> 0.66 us
where the time goes in v3:
time: 70.8 us; the launch traced here: 70.7 us
  Pallas kernels  70 us (99%)
    pallas_call x1, Pallas kernels, local(): pl.pallas_call(functools.partial(kernel, nz, ny, nx), out_shape=vmem((T,...  70 us

profile of v3, /device:TPU:1, one launch (start us, length us, event | category | flops | bytes accessed | tf_op | source)
XLA Modules:
  0.0 70.7 jit_solution(17639437851369809761)
XLA Ops:
  0.0 70.0 %layer.1 = f32[128,256]{1,0:T(8,128)S(1)} custom-call(bf16[128,128]{1,0:T(8,128)(2,1)} %q_hbm.1, bf16[128,128]{1,0:T(8,128)(2,1)} %k_hbm.1, bf16[128,128]{1,0:T(8,128)(2,1)} %v_hbm.1, f32[1,128]{1,0:T(1,128)} %in_hbm.1, f32[1,128]{1,0:T(1,128)} %forget_hbm.1, bf16[128,256]{1,0:T(8,128)(2,1)} %stream_hbm.1, f32[8,128]{1,0:T(8,128)} %bitcast.3, ...), custom_call_target="tpu_custom_call" | custom-call | tf_op jit(solution)/shard_map/layer/pallas_call | solution.py:765
  70.0 0.7 copy.14

commit v4 on v3

--- a/solution.py
+++ b/solution.py
@@ -18,10 +18,11 @@
 EPS = 1e-6
 FAR = -1e30
 SECTION = 4
-TURNS = ((0, 0), (6, 6), (3, 3), (5, 5), (4, 4))
-FIRST = 3
+PIECES = ((0, 0, 32), (0, 32, 32), (0, 64, 32), (0, 96, 32), (1, 0, 96), (1, 96, 80))
+TURNS = ((0, 0), (12, 13), (6, 6), (11, 11), (10, 10))
+FIRST = 4
 GROUPS = (0, 3, 2, 1)
-RING_ROUNDS = (8, 7)
+RING_ROUNDS = (7, 8)
 
 
 def dot(a, b):
@@ -342,9 +343,10 @@
     def ring_part(way, r, m, arriving):
         step = r if arriving else r - 1
         slot = lax.rem(z + step, nz) if way else lax.rem(z + nz - step, nz)
-        ref = w_d.at[slot, pl.ds(0, UNITS)] if m == 2 else gu_rows(slot, m * (T // 2), T // 2)
+        down, begin, count = PIECES[m]
+        ref = w_d.at[slot, pl.ds(begin, count)] if down else gu_rows(slot, begin, count)
         to = down_z if way else up_z
-        return remote(ref, ref, ring_s.at[2 * way + m // 2], ring_r.at[way, m, r], z=to)
+        return remote(ref, ref, ring_s.at[2 * way + down], ring_r.at[way, m, r - 1], z=to)
 
     def lend(slot):
         @pl.when(lax.rem(slot // 2, 2) == other)
@@ -353,16 +355,16 @@
             send(w_d.at[slot, pl.ds(0, UNITS)], there, d2_s, d2_r, c=other)
 
     def ring_begin(way):
-        for m in range(3):
+        for m in range(len(PIECES)):
             ring_part(way, 1, m, False).start()
 
-    turns = [[(way, r, m) for r in range(1, rounds[way] + 1) for m in range(3)] for way in range(2)]
+    turns = [[(way, r, m) for r in range(1, rounds[way] + 1) for m in range(len(PIECES))] for way in range(2)]
 
     def turn(way, r, m):
         ring_part(way, r, m, True).wait_recv()
         if r < rounds[way]:
             ring_part(way, r + 1, m, False).start()
-        if m == 2:
+        if m == len(PIECES) - 1:
             lend(lax.rem(z + r, nz) if way else lax.rem(z + nz - r, nz))
 
     def all_of(up, down):
@@ -470,7 +472,7 @@
         send(heads.at[tp], heads.at[tp], h_s, h_r, x=to // 2, c=to % 2)
 
     both_turns(3)
-    put_off_turns(4, 4)
+    put_off_turns(8, 8)
 
     arrived(heads.at[0 : n_tp - 1], h_s, h_r)
     mixed = stream_ref[...].astype(F32)
@@ -517,37 +519,37 @@
     to_partner(0, 0, ALL, 0)
 
     both_turns(4)
-    put_off_turns(5, 5)
+    put_off_turns(10, 10)
     arrived(squares.at[0:3], as_s, asx_r)
     for e in (1, 3, 2):
         arrived(ra_got.at[0:2], a_s, ax_r.at[e])
         for d in (2, 1, 3):
             there = dict(y=lax.rem(y + d, ny))
             ref = part_of(e, 0, LOW, c)
-            send(ref, ref, f_s, fa_r, **there)
+            send(ref, ref, f_s, fa_r.at[d], **there)
             ref = square_of(e, 0)
             send(ref, ref, as_s, asy_r, **there)
         arrived(ra_got.at[0:2], a_s, ay_r.at[e])
         for d in (2, 1, 3):
             ref = part_of(0, e, HIGH, c)
-            send(ref, ref, f_s2, fb_r, x=lax.rem(x + d, nx))
+            send(ref, ref, f_s2, fb_r.at[d], x=lax.rem(x + d, nx))
         to_partner(e, 0, ALL, 0)
         to_partner(0, e, ALL, 1, False)
     def corners_on():
-        corners = [(dx, dy) for dx in (1, 2, 3) for dy in (1, 2, 3)]
-        arrived(ra_got.at[0:9], f_s, fa_r)
-        for dx, dy in corners:
-            to_partner(dx, dy, LOW, 2, False)
+        for e in (1, 3, 2):
+            arrived(ra_got.at[0:3], f_s, fa_r.at[e])
+            for d in (1, 2, 3):
+                to_partner(d, e, LOW, 2, False)
+            arrived(ra_got.at[0:3], f_s, fb_r.at[e])
+            for d in (1, 2, 3):
+                to_partner(e, d, HIGH, 3, False)
         arrived(squares.at[0:12], as_s, asy_r)
         for dx in range(nx):
             for dy in (1, 2, 3):
                 ref = square_of(dx, dy)
                 send(ref, ref, p_s.at[1], ps_r.at[1], c=other)
-        arrived(ra_got.at[0:9], f_s, fb_r)
-        for dx, dy in corners:
-            to_partner(dx, dy, HIGH, 3, False)
-
-    put_off_turns(7, 7)
+
+    put_off_turns(14, 14)
     pl.when(z < FIRST)(corners_on)
     rest_of_turns()
     lane_wide = lax.broadcasted_iota(jnp.int32, (T, T), 1)
@@ -555,60 +557,72 @@
     def tokens_of(dy):
         return pl.ds(pl.multiple_of(lax.rem(y + ny - dy, ny) * T, T), T)
 
-    def make_hidden(n):
-        dy = GROUPS[n]
-        tokens = tokens_of(dy)
-        total_square = jnp.zeros((1, T), F32)
-        both = jnp.zeros((T, 3 * T), F32)
+    def make_hidden(first, last):
+        groups = range(first, last)
+        both = jnp.zeros(((last - first) * T, 3 * T), F32)
         for b in range(n_tp):
-            total_square = total_square + squares[b * ny + lax.rem(y + ny - dy, ny)][0:1]
-            both = both + dot(acts[b, tokens, :], w_gu[2 * b : 2 * b + 2].reshape(2 * T, 3 * T))
-        factor = lax.rsqrt(column(total_square) * (1.0 / (n_tp * WIDE)) + EPS)
-        both = both * factor
-        gate, up, rest = both[:, 0:T], both[:, T : 2 * T], both[:, 2 * T : 3 * T]
-        here = slice(n * T, (n + 1) * T)
-        hidden[c, here, 0:T] = (gate / (1.0 + jnp.exp(-gate)) * up).astype(BF16)
-        small = rest / (1.0 + jnp.exp(-rest)) * pltpu.roll(rest, 64, 1)
-        hidden[c, here, T : 2 * T] = jnp.where(lane_wide < 48, small, 0.0).astype(BF16)
-        ref = hidden.at[c, here, :]
-        send(ref, ref, x_s, x_r.at[n], c=other)
+            some = [acts[b, tokens_of(GROUPS[n]), :] for n in groups]
+            some = jnp.concatenate(some, axis=0) if len(some) > 1 else some[0]
+            both = both + dot(some, w_gu[2 * b : 2 * b + 2].reshape(2 * T, 3 * T))
+        factors = []
+        for n in groups:
+            total_square = jnp.zeros((1, T), F32)
+            for b in range(n_tp):
+                there = b * ny + lax.rem(y + ny - GROUPS[n], ny)
+                total_square = total_square + squares[there][0:1]
+            factors.append(lax.rsqrt(column(total_square) * (1.0 / (n_tp * WIDE)) + EPS))
+        for n in groups:
+            part = both[(n - first) * T : (n - first + 1) * T] * factors[n - first]
+            gate, up, rest = part[:, 0:T], part[:, T : 2 * T], part[:, 2 * T : 3 * T]
+            here = slice(n * T, (n + 1) * T)
+            hidden[c, here, 0:T] = (gate / (1.0 + jnp.exp(-gate)) * up).astype(BF16)
+            small = rest / (1.0 + jnp.exp(-rest)) * pltpu.roll(rest, 64, 1)
+            hidden[c, here, T : 2 * T] = jnp.where(lane_wide < 48, small, 0.0).astype(BF16)
+            ref = hidden.at[c, here, :]
+            send(ref, ref, x_s, x_r.at[n], c=other)
 
     arrived(ra_got.at[0 : 2 * nx], p_s.at[0], p_r.at[0])
     arrived(squares.at[0:nx], p_s.at[1], ps_r.at[0])
-    make_hidden(0)
+    make_hidden(0, 1)
     pl.when(z >= FIRST)(corners_on)
 
     def share_out(first, last):
         for n in range(first, last):
             arrived(hidden.at[other, n * T : (n + 1) * T, :], x_s, x_r.at[n])
         mine, partners = (hidden[core, first * T : last * T, :] for core in (c, other))
-        for dx in (2, 1, 3, 0):
+        def share_of(dx):
             b = lax.rem(x + nx - dx, nx)
             own = jnp.concatenate([w_d[4 * b + 2 * c], w_d[4 * b + 2 * c + 1]], axis=1)
             theirs = jnp.concatenate([w_d2[2 * b], w_d2[2 * b + 1]], axis=1)
-            share = (dot(mine, own) + dot(partners, theirs)).astype(BF16)
+            return (dot(mine, own) + dot(partners, theirs)).astype(BF16)
+
+        def hand_out(dx, share):
             for n in range(first, last):
                 dy = GROUPS[n]
                 at = slice((n - first) * T, (n - first + 1) * T)
-                ra_send[dx * ny + dy] = share[at, 0:T]
-                rb_send[dy * nx + dx] = share[at, T : 2 * T]
+                n_a, n_b = dx * ny + dy, dy * nx + dx
+                ra_send[n_a] = share[at, 0:T]
+                rb_send[n_b] = share[at, T : 2 * T]
                 if dx:
-                    n_a = dx * ny + dy
-                    send(ra_send.at[n_a], ra_got.at[n_a], r_s, ra_r.at[dy], x=b)
-        for n in range(first, last):
-            dy = GROUPS[n]
-            if dy:
-                block = pl.ds(dy * nx, nx)
-                there = dict(y=lax.rem(y + ny - dy, ny))
-                send(rb_send.at[block], rb_got.at[block], rb_s, rb_r, **there)
+                    there = dict(x=lax.rem(x + nx - dx, nx))
+                    send(ra_send.at[n_a], ra_got.at[n_a], r_s, ra_r.at[dy], **there)
+                if dy:
+                    there = dict(y=lax.rem(y + ny - dy, ny))
+                    send(rb_send.at[n_b], rb_got.at[n_b], rb_s, rb_r, **there)
+
+        ready = None
+        for dx in (2, 1, 3, 0):
+            share = share_of(dx)
+            if ready is not None:
+                hand_out(*ready)
+            ready = dx, share
+        hand_out(*ready)
 
     arrived(ra_got.at[0:6], p_s.at[0], p_r.at[1])
     arrived(squares.at[0 : nx * (ny - 1)], p_s.at[1], ps_r.at[1])
     for n in (2, 3):
         arrived(ra_got.at[0:9], p_s.at[0], p_r.at[n])
-    make_hidden(2)
-    make_hidden(3)
-    make_hidden(1)
+    make_hidden(1, 4)
     arrived(w_d2.at[0 : 2 * nx, pl.ds(0, UNITS)], d2_s, d2_r)
     share_out(2, 4)
     share_out(0, 2)
@@ -733,7 +747,7 @@
         dma,
         dma,
         dma((4,)),
-        dma((2, 3, max(RING_ROUNDS) + 1)),
+        dma((2, len(PIECES), max(RING_ROUNDS))),
         dma,
         dma,
         dma,
@@ -744,8 +758,8 @@
         dma,
         dma,
         dma,
-        dma,
-        dma,
+        dma((ny,)),
+        dma((nx,)),
         dma((2,)),
         dma((4,)),
         dma((2,)),

time: 70.8 us -> 67.6 us (0.955)
  Pallas kernels: 70 us -> 66.8 us
    pallas_call x1, Pallas kernels: 70 us -> 66.8 us  [local(): pl.pallas_call(functools.partial(kernel, nz, ny, nx), out_shape=vmem((T,...]
where the time goes in v4:
time: 67.6 us; the launch traced here: 67.4 us
  Pallas kernels  66.8 us (99%)
    pallas_call x1, Pallas kernels, local(): pl.pallas_call(functools.partial(kernel, nz, ny, nx), out_shape=vmem((T,...  66.8 us

profile of v4, /device:TPU:1, one launch (start us, length us, event | category | flops | bytes accessed | tf_op | source)
XLA Modules:
  0.0 67.4 jit_solution(4943955984484460249)
XLA Ops:
  0.0 66.8 %layer.1 = f32[128,256]{1,0:T(8,128)S(1)} custom-call(bf16[128,128]{1,0:T(8,128)(2,1)} %q_hbm.1, bf16[128,128]{1,0:T(8,128)(2,1)} %k_hbm.1, bf16[128,128]{1,0:T(8,128)(2,1)} %v_hbm.1, f32[1,128]{1,0:T(1,128)} %in_hbm.1, f32[1,128]{1,0:T(1,128)} %forget_hbm.1, bf16[128,256]{1,0:T(8,128)(2,1)} %stream_hbm.1, f32[8,128]{1,0:T(8,128)} %bitcast.3, ...), custom_call_target="tpu_custom_call" | custom-call | tf_op jit(solution)/shard_map/layer/pallas_call | solution.py:779
  66.8 0.7 copy.14
